TPU v7x, 512 devices: a whole 4x4x16 slice. The times are simulated.
512 devices in a mesh: kv: 64 (over z, y), tp: 8 (over x, core).
Axes of the slice: x: 4, y: 4, z: 16, core: 2. Of those that a mesh axis runs over, the one named last changes fastest.
Arguments:
- tokens: bfloat16 [24, 4096], P(None, 'kv'), may hold values from -60 to 60
- gain_first: bfloat16 [4096], P('kv'), may hold values from 0.099609375 to 1.8984375
- gate_first: bfloat16 [4096, 11264], P('kv', 'tp'), may hold values from -0.09375 to 0.09375
- up_first: bfloat16 [4096, 11264], P('kv', 'tp'), may hold values from -0.09375 to 0.09375
- down_first: bfloat16 [11264, 4096], P('tp', 'kv'), may hold values from -0.0546875 to 0.0546875
- gain_mixer: bfloat16 [4096], P('kv'), may hold values from 0.099609375 to 1.8984375
- query_weight: bfloat16 [4096, 2048], P('kv', 'tp'), may hold values from -0.09375 to 0.09375
- key_weight: bfloat16 [4096, 2048], P('kv', 'tp'), may hold values from -0.25 to 0.25
- value_weight: bfloat16 [4096, 2048], P('kv', 'tp'), may hold values from -0.09375 to 0.09375
- forget_weight: bfloat16 [4096, 16], replicated, may hold values from -0.09375 to 0.09375
- forget_bias: float32 [16], replicated, may hold values from -1 to 2
- key_cache: bfloat16 [24, 8192, 16, 128], P(None, 'kv', 'tp'), may hold values from -2000 to 2000
- value_cache: bfloat16 [24, 8192, 16, 128], P(None, 'kv', 'tp'), may hold values from -6 to 6
- forget_sum: float32 [24, 16, 8192], P(None, 'tp', 'kv'), may hold values from -1024 to 0, as said below
- out_weight: bfloat16 [2048, 4096], P('tp', 'kv'), may hold values from -0.5 to 0.5
- gain_second: bfloat16 [4096], P('kv'), may hold values from 0.099609375 to 1.8984375
- gate_second: bfloat16 [4096, 11264], P('kv', 'tp'), may hold values from -0.09375 to 0.09375
- up_second: bfloat16 [4096, 11264], P('kv', 'tp'), may hold values from -0.09375 to 0.09375
- down_second: bfloat16 [11264, 4096], P('tp', 'kv'), may hold values from -0.0546875 to 0.0546875
Outputs:
- updated: bfloat16 [24, 4096], P(None, 'kv')
Inputs may be any that keep to these rules, and one draw needn't show every extreme that they name: forget_sum[b, h, s] is the sum of the log forget gates of the cached positions after s, up to the last cached one, for sequence b and head h; it never falls with s, is at most 0, and rises to 0 at the last cached position.
All inputs are finite; a program needn't handle non-finite values.
Results may differ from a plain program's by a relative error of at most 0.02.
Values may be sent and summed in bfloat16 or wider, within the bound.
A program may use at most 64 MiB of HBM per device.

v0:
```python
import jax
import jax.numpy as jnp
from jax import lax
from jax.sharding import Mesh
from jax.sharding import PartitionSpec as P

D = 4096
BLOCK = 128
KV = ("kv_0", "kv_1")


EPSILON = 1e-06


def split_up(value, dim, count):
    dims = value.shape
    tiles = value.reshape(*dims[:dim], count, dims[dim] // count, *dims[dim + 1 :])
    return jnp.moveaxis(tiles, dim, 0)


def summed_on_arrival(value, axis, dim):
    tiles = split_up(value, dim, lax.axis_size(axis))
    arrived = lax.all_to_all(tiles, axis, split_axis=0, concat_axis=0, tiled=True)
    return arrived.sum(axis=0)


def sum_in_two_steps(value, axes, dim):
    far, near = axes
    own = summed_on_arrival(split_up(value, dim, lax.axis_size(far)), near, dim + 1)
    return jnp.sum(lax.all_to_all(own, far, 0, 0, tiled=True), axis=0)


def sent_to_all(value, axis):
    copies = jnp.broadcast_to(value, (lax.axis_size(axis), *value.shape))
    return lax.all_to_all(copies, axis, split_axis=0, concat_axis=0, tiled=True)


def joined_along(tiles, dim):
    tiles = jnp.moveaxis(tiles, 0, dim)
    dims = tiles.shape
    return tiles.reshape(*dims[:dim], dims[dim] * dims[dim + 1], *dims[dim + 2 :])


def collect(value, axis, dim):
    tiles = sent_to_all(value, axis)
    return joined_along(tiles, dim)


def taken_together(value, axis):
    everything = sent_to_all(value, axis)
    return jnp.sum(everything.astype(jnp.float32), axis=0)


def padded_to(lines, count):
    spare = -len(lines) % count
    return jnp.pad(lines, [(0, spare)] + [(0, 0)] * (lines.ndim - 1))


def total_of(value, axes):
    own = summed_on_arrival(padded_to(value, lax.axis_size(axes)), axes, 0)
    whole = collect(own, axes, 0)
    return whole[: len(value)].reshape(value.shape)


def in_one(arrays, axis):
    ends = [0]
    for a in arrays:
        ends.append(ends[-1] + a.size)
    running = total_of(jnp.concatenate([a.ravel() for a in arrays]), axis)
    return tuple((running[b:e].reshape(a.shape) for a, b, e in zip(arrays, ends, ends[1:])))


def all_in_one(value, axis):
    leaves = jax.tree.leaves(value)
    sequence = sorted(range(len(leaves)), key=lambda k: -leaves[k].size)
    width = (1, *leaves[sequence[0]].shape)[-1]
    lines = [
        jnp.pad(leaves[k].reshape(-1), (0, -leaves[k].size % width)).reshape(-1, width)
        for k in sequence
    ]
    both, at, found = (lax.all_gather(jnp.concatenate(lines), axis), 0, {})
    for k, line in zip(sequence, lines):
        share = both[:, at : at + len(line)].reshape(len(both), -1)
        found[k] = share[:, : leaves[k].size].reshape(-1, *leaves[k].shape)
        at += len(line)
    numbers = iter(range(len(leaves)))
    return jax.tree.map(lambda _: found[next(numbers)], value)


def merged_by_axis(value, axes, combine):
    for axis in axes:
        pieces = all_in_one(value, axis)
        value = jax.tree.map(lambda part: part[0], pieces)
        for k in range(1, lax.axis_size(axis)):
            value = combine(value, jax.tree.map(lambda part: part[k], pieces))
    return value


def merge_parts(former, latter):
    highest = jnp.maximum(former[0], latter[0])
    left_scale = jnp.exp(former[0] - highest)
    right_scale = jnp.exp(latter[0] - highest)
    return (
        highest,
        former[1] * left_scale + latter[1] * right_scale,
        former[2] * left_scale[..., None] + latter[2] * right_scale[..., None],
    )


def row_factor(squares):
    return lax.rsqrt(squares / D + EPSILON)[:, None]


def feed_forward(tokens, norm_gain, gate_matrix, up_matrix, down_matrix):
    widened = tokens.astype(jnp.float32)
    squares = jnp.sum(widened * widened, axis=1)
    scaled = (widened * norm_gain.astype(jnp.float32)).astype(jnp.bfloat16)
    products = jnp.stack(
        [
            jnp.dot(scaled, gate_matrix, preferred_element_type=jnp.float32),
            jnp.dot(scaled, up_matrix, preferred_element_type=jnp.float32),
        ]
    )
    members = lax.axis_size(KV)
    spread = jnp.broadcast_to(squares[None, :, None], (1, squares.shape[0], members))
    products, spread = (
        sum_in_two_steps(products, ("kv_0", "kv_1"), 2),
        sum_in_two_steps(spread, ("kv_0", "kv_1"), 2),
    )
    factor = row_factor(spread[0, :, 0])
    unit_share = (jax.nn.silu(factor * products[0]) * (factor * products[1])).astype(jnp.bfloat16)
    partial_value = jnp.dot(
        collect(unit_share, KV, 1), down_matrix, preferred_element_type=jnp.float32
    )
    summed = taken_together(partial_value.astype(jnp.bfloat16), "tp").astype(jnp.float32)
    return (widened + 0.5 * summed).astype(jnp.bfloat16)


def mix_tokens(
    tokens,
    norm_gain,
    query_weight,
    key_weight,
    value_weight,
    forget_weight,
    forget_bias,
    key_cache,
    value_cache,
    forget_sum,
    out_weight,
):
    widened = tokens.astype(jnp.float32)
    squares = jnp.sum(widened * widened, axis=1)
    scaled = (widened * norm_gain.astype(jnp.float32)).astype(jnp.bfloat16)
    columns = scaled.shape[1]
    forget_rows = lax.dynamic_slice_in_dim(forget_weight, lax.axis_index(KV) * columns, columns, 0)
    triple = jnp.stack(
        [
            jnp.dot(scaled, query_weight, preferred_element_type=jnp.float32),
            jnp.dot(scaled, key_weight, preferred_element_type=jnp.float32),
            jnp.dot(scaled, value_weight, preferred_element_type=jnp.float32),
        ]
    )
    gate_terms = jnp.dot(scaled, forget_rows, preferred_element_type=jnp.float32)
    triple, gate_terms, squares = in_one((triple, gate_terms, squares), KV)
    factor = row_factor(squares)
    seq_count = tokens.shape[0]
    local_heads = key_cache.shape[2]
    head_size = key_cache.shape[3]
    shaped = (
        (factor[None] * triple).astype(jnp.bfloat16).reshape(3, seq_count, local_heads, head_size)
    )
    query_rows, new_key, new_value = (shaped[0], shaped[1], shaped[2])
    all_gates = jax.nn.log_sigmoid(factor * gate_terms + forget_bias)
    log_gate = lax.dynamic_slice_in_dim(
        all_gates, lax.axis_index("tp") * local_heads, local_heads, 1
    )
    inverse = head_size ** (-0.5)
    scores = (
        jnp.einsum("bhd,bshd->bhs", query_rows, key_cache, preferred_element_type=jnp.float32)
        * inverse
    )
    scores = scores + forget_sum + log_gate[:, :, None]
    blocks = key_cache.shape[1] // BLOCK
    scores = scores.reshape(seq_count, local_heads, blocks, BLOCK)
    highest = jnp.max(scores, axis=3)
    weights = jnp.exp(scores - highest[..., None]).astype(jnp.bfloat16)
    block_sum = jnp.sum(weights.astype(jnp.float32), axis=3)
    block_value = jnp.einsum(
        "bhcs,bcshd->bhcd",
        weights,
        value_cache.reshape(seq_count, blocks, BLOCK, local_heads, head_size),
        preferred_element_type=jnp.float32,
    )
    local_top = jnp.max(highest, axis=2)
    rescale = jnp.exp(highest - local_top[..., None])
    denominator = jnp.sum(rescale * block_sum, axis=2)
    numerator = jnp.sum(rescale[..., None] * block_value, axis=2)
    local_top, denominator, numerator = merged_by_axis(
        (local_top, denominator, numerator), KV, merge_parts
    )
    own_score = (
        jnp.sum(query_rows.astype(jnp.float32) * new_key.astype(jnp.float32), axis=2) * inverse
    )
    ceiling = jnp.maximum(local_top, own_score)
    cache_scale = jnp.exp(local_top - ceiling)
    own_scale = jnp.exp(own_score - ceiling)
    attended = (
        (numerator * cache_scale[..., None] + own_scale[..., None] * new_value.astype(jnp.float32))
        / (denominator * cache_scale + own_scale)[..., None]
    ).astype(jnp.bfloat16)
    partial_value = jnp.dot(
        attended.reshape(seq_count, local_heads * head_size),
        out_weight,
        preferred_element_type=jnp.float32,
    )
    summed = taken_together(partial_value.astype(jnp.bfloat16), "tp").astype(jnp.float32)
    return (widened + summed).astype(jnp.bfloat16)


def on_device(
    tokens,
    gain_first,
    gate_first,
    up_first,
    down_first,
    gain_mixer,
    query_weight,
    key_weight,
    value_weight,
    forget_weight,
    forget_bias,
    key_cache,
    value_cache,
    forget_sum,
    out_weight,
    gain_second,
    gate_second,
    up_second,
    down_second,
):
    first_out = feed_forward(tokens, gain_first, gate_first, up_first, down_first)
    mixed = mix_tokens(
        first_out,
        gain_mixer,
        query_weight,
        key_weight,
        value_weight,
        forget_weight,
        forget_bias,
        key_cache,
        value_cache,
        forget_sum,
        out_weight,
    )
    return feed_forward(mixed, gain_second, gate_second, up_second, down_second)


def solution(mesh):
    split = Mesh(mesh.devices.reshape(16, 4, mesh.shape["tp"]), ("kv_0", "kv_1", "tp"))
    in_specs = (
        P(None, KV),
        P(KV),
        P(KV, "tp"),
        P(KV, "tp"),
        P("tp", KV),
        P(KV),
        P(KV, "tp"),
        P(KV, "tp"),
        P(KV, "tp"),
        P(),
        P(),
        P(None, KV, "tp", None),
        P(None, KV, "tp", None),
        P(None, "tp", KV),
        P("tp", KV),
        P(KV),
        P(KV, "tp"),
        P(KV, "tp"),
        P("tp", KV),
    )
    out_specs = P(None, KV)
    return jax.shard_map(
        on_device, mesh=split, in_specs=in_specs, out_specs=out_specs, check_vma=False
    )
```

profile of v0, /device:TPU:1, one launch (start us, length us, event | category | flops | bytes accessed | tf_op | source)
XLA Modules:
  0.0 294.9 jit_solution(15402023415753041623)
XLA Ops:
  0.0 0.9 fusion.57
  0.9 0.7 reshape.1634
  1.6 5.0 %all-to-all-start = ((f32[4,1,384]{2,1,0:T(1,128)}), f32[4,1,384]{2,1,0:T(1,128)S(1)}, u32[]{:S(2)}, u32[]{:S(2)}) async-start(f32[4,1,384]{2,1,0:T(1,128)} %reshape.1634), calls=%async_computation | async-start | bytes 12288 | tf_op jit(solution)/shard_map/all_to_all | solution.py:23
  6.6 0.7 convert_element_type.107
  7.3 1.1 fusion.84
  8.6 1.1 fusion.86
  10.0 0.7 reshape.1552
  10.7 2.0 copy.68
  12.7 3.1 %reshape.1630 = f32[4,1,16896]{2,1,0:T(1,128)} reshape(f32[4,2,22,16,24]{4,3,2,1,0:T(8,128)} %bitcast.677) | data formatting | bytes 540672
  15.9 4.2 %all-to-all-start.2 = ((f32[4,1,16896]{2,1,0:T(1,128)}), f32[4,1,16896]{2,1,0:T(1,128)S(1)}, u32[]{:S(2)}, u32[]{:S(2)}) async-start(f32[4,1,16896]{2,1,0:T(1,128)} %reshape.1630), calls=%async_computation.2 | async-start | bytes 540672 | tf_op jit(solution)/shard_map/all_to_all | solution.py:23
  20.1 0.6 broadcast.163
  20.7 0.7 reduce.45
  21.5 0.6 bitcast_reduce_fusion.5
  22.1 3.6 %all-to-all-done.2 = f32[4,1,16896]{2,1,0:T(1,128)S(1)} async-done(((f32[4,1,16896]{2,1,0:T(1,128)}), f32[4,1,16896]{2,1,0:T(1,128)S(1)}, u32[]{:S(2)}, u32[]{:S(2)}) %all-to-all-start.2) | async-done | bytes 270368 | tf_op jit(solution)/shard_map/all_to_all | solution.py:23
  25.7 14.9 %all-to-all-start.1 = ((f32[16,1,24,1]{2,3,1,0:T(1,128)}), f32[16,1,24,1]{2,3,1,0:T(1,128)S(1)}, u32[]{:S(2)}, u32[]{:S(2)}) async-start(f32[16,1,24,1]{2,3,1,0:T(1,128)} %bitcast), calls=%async_computation.1 | async-start | bytes 16384 | tf_op jit(solution)/shard_map/all_to_all | solution.py:30
  40.6 1.4 reduce.43
  42.0 1.1 reshape.1631
  43.5 1.0 reshape.1632
  44.5 7.3 %all-to-all-done.1 = f32[16,1,24,1]{2,3,1,0:T(1,128)S(1)} async-done(((f32[16,1,24,1]{2,3,1,0:T(1,128)}), f32[16,1,24,1]{2,3,1,0:T(1,128)S(1)}, u32[]{:S(2)}, u32[]{:S(2)}) %all-to-all-start.1) | async-done | bytes 1568 | tf_op jit(solution)/shard_map/all_to_all | solution.py:30
  51.8 4.2 %all-to-all-start.3 = ((f32[16,1,1056]{2,1,0:T(1,128)}), f32[16,1,1056]{2,1,0:T(1,128)S(1)}, u32[]{:S(2)}, u32[]{:S(2)}) async-start(f32[16,1,1056]{2,1,0:T(1,128)} %reshape.1632), calls=%async_computation.3 | async-start | bytes 147456 | tf_op jit(solution)/shard_map/all_to_all | solution.py:30
  56.1 11.7 %all-to-all-done.3 = f32[16,1,1056]{2,1,0:T(1,128)S(1)} async-done(((f32[16,1,1056]{2,1,0:T(1,128)}), f32[16,1,1056]{2,1,0:T(1,128)S(1)}, u32[]{:S(2)}, u32[]{:S(2)}) %all-to-all-start.3) | async-done | bytes 67616 | tf_op jit(solution)/shard_map/all_to_all | solution.py:30
  67.7 0.8 reduce.44
  69.3 0.5 reshape.1636
  69.8 19.0 %all_to_all.80 = bf16[64,2,264]{2,1,0:T(2,128)(2,1)S(1)} all-to-all(bf16[64,2,264]{2,1,0:T(2,128)(2,1)S(1)} %reshape.1636), channel_id=1, replica_groups=mesh['kv_0'=16,'kv_1'=4,'tp'=8] {'kv_0','kv_1'}, dimensions={0} | all-to-all | bytes 135168 | tf_op jit(solution)/shard_map/all_to_all | solution.py:35
  88.8 0.4 reshape.1637
  89.3 0.5 reshape.1553
  90.0 0.7 reshape.1638
  90.7 10.0 %all-to-all-start.5 = ((bf16[8,2,768]{2,1,0:T(2,128)(2,1)}), bf16[8,2,768]{2,1,0:T(2,128)(2,1)S(1)}, u32[]{:S(2)}, u32[]{:S(2)}) async-start(bf16[8,2,768]{2,1,0:T(2,128)(2,1)} %reshape.1638), calls=%async_computation.5 | async-start | bytes 49152 | tf_op jit(solution)/shard_map/all_to_all | solution.py:35
  100.8 4.7 %all-to-all-done.5 = bf16[8,2,768]{2,1,0:T(2,128)(2,1)S(1)} async-done(((bf16[8,2,768]{2,1,0:T(2,128)(2,1)}), bf16[8,2,768]{2,1,0:T(2,128)(2,1)S(1)}, u32[]{:S(2)}, u32[]{:S(2)}) %all-to-all-start.5) | async-done | bytes 24608 | tf_op jit(solution)/shard_map/all_to_all | solution.py:35
  105.7 0.9 fusion.88
  107.4 18.6 %all_to_all.81 = f32[64,1,295]{2,1,0:T(1,128)S(1)} all-to-all(f32[64,1,295]{2,1,0:T(1,128)S(1)} %all_to_all.55), channel_id=1, replica_groups=mesh['kv_0'=16,'kv_1'=4,'tp'=8] {'kv_0','kv_1'}, dimensions={0} | all-to-all | bytes 151040 | tf_op jit(solution)/shard_map/all_to_all | solution.py:23
  126.1 0.7 broadcast_in_dim.14
  126.8 5.2 %all-to-all-start.7 = ((f32[64,1,295]{2,1,0:T(1,128)}), f32[64,1,295]{2,1,0:T(1,128)S(1)}, u32[]{:S(2)}, u32[]{:S(2)}) async-start(f32[64,1,295]{2,1,0:T(1,128)} %broadcast_in_dim.14), calls=%async_computation.7 | async-start | bytes 196608 | tf_op jit(solution)/shard_map/all_to_all | solution.py:35
  132.0 14.5 %all-to-all-done.7 = f32[64,1,295]{2,1,0:T(1,128)S(1)} async-done(((f32[64,1,295]{2,1,0:T(1,128)}), f32[64,1,295]{2,1,0:T(1,128)S(1)}, u32[]{:S(2)}, u32[]{:S(2)}) %all-to-all-start.7) | async-done | bytes 75552 | tf_op jit(solution)/shard_map/all_to_all | solution.py:35
  147.1 0.4 slice.363
  147.5 0.9 fusion.2
  149.2 1.9 fusion
  151.3 22.9 %all-gather.2 = f32[16,50,128]{2,1,0:T(8,128)S(1)} all-gather(f32[1,50,128]{2,1,0:T(8,128)S(1)} %maximum_bitcast_fusion.2), channel_id=2, replica_groups=mesh['kv_0'=16,'kv_1'=4,'tp'=8] {'kv_0'}, dimensions={0}, use_global_device_ids=true | all-gather | bytes 435200 | tf_op jit(solution)/shard_map/all_gather | solution.py:81
  174.6 9.1 %all-gather.3 = f32[4,50,128]{2,1,0:T(8,128)S(1)} all-gather(f32[1,50,128]{2,1,0:T(8,128)S(1)} %maximum_bitcast_fusion.3), channel_id=3, replica_groups=mesh['kv_0'=16,'kv_1'=4,'tp'=8] {'kv_1'}, dimensions={0}, use_global_device_ids=true | all-gather | bytes 128000 | tf_op jit(solution)/shard_map/all_gather | solution.py:81
  185.8 0.7 reshape.1640
  186.5 15.8 %all-to-all-start.8 = ((bf16[8,2,768]{2,1,0:T(2,128)(2,1)}), bf16[8,2,768]{2,1,0:T(2,128)(2,1)S(1)}, u32[]{:S(2)}, u32[]{:S(2)}) async-start(bf16[8,2,768]{2,1,0:T(2,128)(2,1)} %reshape.1640), calls=%async_computation.8 | async-start | bytes 49152 | tf_op jit(solution)/shard_map/all_to_all | solution.py:35
  202.3 4.7 %all-to-all-done.8 = bf16[8,2,768]{2,1,0:T(2,128)(2,1)S(1)} async-done(((bf16[8,2,768]{2,1,0:T(2,128)(2,1)}), bf16[8,2,768]{2,1,0:T(2,128)(2,1)S(1)}, u32[]{:S(2)}, u32[]{:S(2)}) %all-to-all-start.8) | async-done | bytes 24608 | tf_op jit(solution)/shard_map/all_to_all | solution.py:35
  207.3 0.7 reshape.1646
  208.0 3.2 %all-to-all-start.9 = ((f32[4,1,384]{2,1,0:T(1,128)}), f32[4,1,384]{2,1,0:T(1,128)S(1)}, u32[]{:S(2)}, u32[]{:S(2)}) async-start(f32[4,1,384]{2,1,0:T(1,128)} %reshape.1646), calls=%async_computation.9 | async-start | bytes 12288 | tf_op jit(solution)/shard_map/all_to_all | solution.py:23
  212.1 0.7 reshape.1568
  212.8 2.0 copy.77
  214.8 3.1 %reshape.1642 = f32[4,1,16896]{2,1,0:T(1,128)} reshape(f32[4,2,22,16,24]{4,3,2,1,0:T(8,128)} %bitcast.678) | data formatting | bytes 540672
  217.9 4.2 %all-to-all-start.11 = ((f32[4,1,16896]{2,1,0:T(1,128)}), f32[4,1,16896]{2,1,0:T(1,128)S(1)}, u32[]{:S(2)}, u32[]{:S(2)}) async-start(f32[4,1,16896]{2,1,0:T(1,128)} %reshape.1642), calls=%async_computation.11 | async-start | bytes 540672 | tf_op jit(solution)/shard_map/all_to_all | solution.py:23
  222.1 0.7 reduce.48
  222.9 0.6 bitcast_reduce_fusion.4
  223.5 4.2 %all-to-all-done.11 = f32[4,1,16896]{2,1,0:T(1,128)S(1)} async-done(((f32[4,1,16896]{2,1,0:T(1,128)}), f32[4,1,16896]{2,1,0:T(1,128)S(1)}, u32[]{:S(2)}, u32[]{:S(2)}) %all-to-all-start.11) | async-done | bytes 270368 | tf_op jit(solution)/shard_map/all_to_all | solution.py:23
  227.7 4.4 %all-to-all-start.10 = ((f32[16,1,24,1]{2,3,1,0:T(1,128)}), f32[16,1,24,1]{2,3,1,0:T(1,128)S(1)}, u32[]{:S(2)}, u32[]{:S(2)}) async-start(f32[16,1,24,1]{2,3,1,0:T(1,128)} %bitcast.73), calls=%async_computation.10 | async-start | bytes 16384 | tf_op jit(solution)/shard_map/all_to_all | solution.py:30
  232.1 1.4 reduce.46
  233.6 1.1 reshape.1643
  235.0 1.0 reshape.1644
  236.1 7.3 %all-to-all-done.10 = f32[16,1,24,1]{2,3,1,0:T(1,128)S(1)} async-done(((f32[16,1,24,1]{2,3,1,0:T(1,128)}), f32[16,1,24,1]{2,3,1,0:T(1,128)S(1)}, u32[]{:S(2)}, u32[]{:S(2)}) %all-to-all-start.10) | async-done | bytes 1568 | tf_op jit(solution)/shard_map/all_to_all | solution.py:30
  243.4 4.1 %all-to-all-start.12 = ((f32[16,1,1056]{2,1,0:T(1,128)}), f32[16,1,1056]{2,1,0:T(1,128)S(1)}, u32[]{:S(2)}, u32[]{:S(2)}) async-start(f32[16,1,1056]{2,1,0:T(1,128)} %reshape.1644), calls=%async_computation.12 | async-start | bytes 147456 | tf_op jit(solution)/shard_map/all_to_all | solution.py:30
  247.6 11.7 %all-to-all-done.12 = f32[16,1,1056]{2,1,0:T(1,128)S(1)} async-done(((f32[16,1,1056]{2,1,0:T(1,128)}), f32[16,1,1056]{2,1,0:T(1,128)S(1)}, u32[]{:S(2)}, u32[]{:S(2)}) %all-to-all-start.12) | async-done | bytes 67616 | tf_op jit(solution)/shard_map/all_to_all | solution.py:30
  259.2 0.9 reduce.47
  260.8 0.5 reshape.1648
  261.3 19.0 %all_to_all.82 = bf16[64,2,264]{2,1,0:T(2,128)(2,1)S(1)} all-to-all(bf16[64,2,264]{2,1,0:T(2,128)(2,1)S(1)} %reshape.1648), channel_id=1, replica_groups=mesh['kv_0'=16,'kv_1'=4,'tp'=8] {'kv_0','kv_1'}, dimensions={0} | all-to-all | bytes 135168 | tf_op jit(solution)/shard_map/all_to_all | solution.py:35
  280.8 0.5 reshape.1569
  281.6 12.5 %all_to_all.83 = bf16[8,2,768]{2,1,0:T(2,128)(2,1)S(1)} all-to-all(bf16[8,2,768]{2,1,0:T(2,128)(2,1)S(1)} %reshape.1650), channel_id=1, replica_groups=mesh['kv_0'=16,'kv_1'=4,'tp'=8] {'tp'}, dimensions={0} | all-to-all | bytes 49152 | tf_op jit(solution)/shard_map/all_to_all | solution.py:35
  294.3 0.6 fusion.65
  (150 shorter events, 10.1 us)
Async XLA Ops:
  0.0 147.5 %copy-start = (bf16[24,128,2,128]{3,2,1,0:T(2,128)(2,1)S(1)}, bf16[24,128,2,128]{3,2,1,0:T(2,128)(2,1)}, u32[]{:S(2)}) copy-start(bf16[24,128,2,128]{3,2,1,0:T(2,128)(2,1)} %param.30) | copy-start | bytes 4718596
  1.6 14.2 %all-to-all-start = ((f32[4,1,384]{2,1,0:T(1,128)}), f32[4,1,384]{2,1,0:T(1,128)S(1)}, u32[]{:S(2)}, u32[]{:S(2)}) async-start(f32[4,1,384]{2,1,0:T(1,128)} %reshape.1634), calls=%async_computation | async-start | bytes 12288 | tf_op jit(solution)/shard_map/all_to_all | solution.py:23
  15.9 9.8 %all-to-all-start.2 = ((f32[4,1,16896]{2,1,0:T(1,128)}), f32[4,1,16896]{2,1,0:T(1,128)S(1)}, u32[]{:S(2)}, u32[]{:S(2)}) async-start(f32[4,1,16896]{2,1,0:T(1,128)} %reshape.1630), calls=%async_computation.2 | async-start | bytes 540672 | tf_op jit(solution)/shard_map/all_to_all | solution.py:23
  25.7 26.2 %all-to-all-start.1 = ((f32[16,1,24,1]{2,3,1,0:T(1,128)}), f32[16,1,24,1]{2,3,1,0:T(1,128)S(1)}, u32[]{:S(2)}, u32[]{:S(2)}) async-start(f32[16,1,24,1]{2,3,1,0:T(1,128)} %bitcast), calls=%async_computation.1 | async-start | bytes 16384 | tf_op jit(solution)/shard_map/all_to_all | solution.py:30
  51.8 15.9 %all-to-all-start.3 = ((f32[16,1,1056]{2,1,0:T(1,128)}), f32[16,1,1056]{2,1,0:T(1,128)S(1)}, u32[]{:S(2)}, u32[]{:S(2)}) async-start(f32[16,1,1056]{2,1,0:T(1,128)} %reshape.1632), calls=%async_computation.3 | async-start | bytes 147456 | tf_op jit(solution)/shard_map/all_to_all | solution.py:30
  68.9 20.9 %copy-start.3 = (bf16[1408,64]{0,1:T(8,128)(2,1)S(1)}, bf16[1408,64]{0,1:T(8,128)(2,1)}, u32[]{:S(2)}) copy-start(bf16[1408,64]{0,1:T(8,128)(2,1)} %param.23) | copy-start | bytes 540676
  69.2 31.5 %copy-start.12 = (bf16[64]{0:T(256)(128)(2,1)S(1)}, bf16[64]{0:T(256)(128)(2,1)}, u32[]{:S(2)}) copy-start(bf16[64]{0:T(256)(128)(2,1)} %param.24) | copy-start | bytes 388
  69.3 36.3 %copy-start.6 = (bf16[24,64]{1,0:T(8,128)(2,1)S(1)}, bf16[24,64]{1,0:T(8,128)(2,1)}, u32[]{:S(2)}) copy-start(bf16[24,64]{1,0:T(8,128)(2,1)} %param.19) | copy-start | bytes 9220
  69.3 37.4 %copy-start.8 = (bf16[64,256]{1,0:T(8,128)(2,1)S(1)}, bf16[64,256]{1,0:T(8,128)(2,1)}, u32[]{:S(2)}) copy-start(bf16[64,256]{1,0:T(8,128)(2,1)} %param.27) | copy-start | bytes 98308
  69.3 37.5 %copy-start.9 = (bf16[64,256]{1,0:T(8,128)(2,1)S(1)}, bf16[64,256]{1,0:T(8,128)(2,1)}, u32[]{:S(2)}) copy-start(bf16[64,256]{1,0:T(8,128)(2,1)} %param.26) | copy-start | bytes 98308
  69.3 37.6 %copy-start.10 = (bf16[64,256]{1,0:T(8,128)(2,1)S(1)}, bf16[64,256]{1,0:T(8,128)(2,1)}, u32[]{:S(2)}) copy-start(bf16[64,256]{1,0:T(8,128)(2,1)} %param.25) | copy-start | bytes 98308
  90.7 14.7 %all-to-all-start.5 = ((bf16[8,2,768]{2,1,0:T(2,128)(2,1)}), bf16[8,2,768]{2,1,0:T(2,128)(2,1)S(1)}, u32[]{:S(2)}, u32[]{:S(2)}) async-start(bf16[8,2,768]{2,1,0:T(2,128)(2,1)} %reshape.1638), calls=%async_computation.5 | async-start | bytes 49152 | tf_op jit(solution)/shard_map/all_to_all | solution.py:35
  126.8 19.7 %all-to-all-start.7 = ((f32[64,1,295]{2,1,0:T(1,128)}), f32[64,1,295]{2,1,0:T(1,128)S(1)}, u32[]{:S(2)}, u32[]{:S(2)}) async-start(f32[64,1,295]{2,1,0:T(1,128)} %broadcast_in_dim.14), calls=%async_computation.7 | async-start | bytes 196608 | tf_op jit(solution)/shard_map/all_to_all | solution.py:35
  131.9 16.4 %copy-start.11 = (f32[16]{0:T(128)S(1)}, f32[16]{0:T(128)}, u32[]{:S(2)}) copy-start(f32[16]{0:T(128)} %param.29) | copy-start | bytes 196
  146.7 1.9 copy-start.5
  151.1 34.5 %copy-start.7 = (bf16[256,64]{0,1:T(8,128)(2,1)S(1)}, bf16[256,64]{0,1:T(8,128)(2,1)}, u32[]{:S(2)}) copy-start(bf16[256,64]{0,1:T(8,128)(2,1)} %param.33) | copy-start | bytes 98308
  151.2 51.1 %copy-start.13 = (bf16[64]{0:T(256)(128)(2,1)S(1)}, bf16[64]{0:T(256)(128)(2,1)}, u32[]{:S(2)}) copy-start(bf16[64]{0:T(256)(128)(2,1)} %param.34) | copy-start | bytes 388
  151.3 60.0 %copy-start.1 = (bf16[64,1408]{1,0:T(8,128)(2,1)S(1)}, bf16[64,1408]{1,0:T(8,128)(2,1)}, u32[]{:S(2)}) copy-start(bf16[64,1408]{1,0:T(8,128)(2,1)} %param.35) | copy-start | bytes 540676
  183.7 27.9 %copy-start.2 = (bf16[64,1408]{1,0:T(8,128)(2,1)S(1)}, bf16[64,1408]{1,0:T(8,128)(2,1)}, u32[]{:S(2)}) copy-start(bf16[64,1408]{1,0:T(8,128)(2,1)} %param.36) | copy-start | bytes 540676
  186.5 20.5 %all-to-all-start.8 = ((bf16[8,2,768]{2,1,0:T(2,128)(2,1)}), bf16[8,2,768]{2,1,0:T(2,128)(2,1)S(1)}, u32[]{:S(2)}, u32[]{:S(2)}) async-start(bf16[8,2,768]{2,1,0:T(2,128)(2,1)} %reshape.1640), calls=%async_computation.8 | async-start | bytes 49152 | tf_op jit(solution)/shard_map/all_to_all | solution.py:35
  208.0 10.0 %all-to-all-start.9 = ((f32[4,1,384]{2,1,0:T(1,128)}), f32[4,1,384]{2,1,0:T(1,128)S(1)}, u32[]{:S(2)}, u32[]{:S(2)}) async-start(f32[4,1,384]{2,1,0:T(1,128)} %reshape.1646), calls=%async_computation.9 | async-start | bytes 12288 | tf_op jit(solution)/shard_map/all_to_all | solution.py:23
  217.9 9.8 %all-to-all-start.11 = ((f32[4,1,16896]{2,1,0:T(1,128)}), f32[4,1,16896]{2,1,0:T(1,128)S(1)}, u32[]{:S(2)}, u32[]{:S(2)}) async-start(f32[4,1,16896]{2,1,0:T(1,128)} %reshape.1642), calls=%async_computation.11 | async-start | bytes 540672 | tf_op jit(solution)/shard_map/all_to_all | solution.py:23
  227.7 15.7 %all-to-all-start.10 = ((f32[16,1,24,1]{2,3,1,0:T(1,128)}), f32[16,1,24,1]{2,3,1,0:T(1,128)S(1)}, u32[]{:S(2)}, u32[]{:S(2)}) async-start(f32[16,1,24,1]{2,3,1,0:T(1,128)} %bitcast.73), calls=%async_computation.10 | async-start | bytes 16384 | tf_op jit(solution)/shard_map/all_to_all | solution.py:30
  243.4 15.9 %all-to-all-start.12 = ((f32[16,1,1056]{2,1,0:T(1,128)}), f32[16,1,1056]{2,1,0:T(1,128)S(1)}, u32[]{:S(2)}, u32[]{:S(2)}) async-start(f32[16,1,1056]{2,1,0:T(1,128)} %reshape.1644), calls=%async_computation.12 | async-start | bytes 147456 | tf_op jit(solution)/shard_map/all_to_all | solution.py:30
  260.4 20.9 %copy-start.4 = (bf16[1408,64]{0,1:T(8,128)(2,1)S(1)}, bf16[1408,64]{0,1:T(8,128)(2,1)}, u32[]{:S(2)}) copy-start(bf16[1408,64]{0,1:T(8,128)(2,1)} %param.37) | copy-start | bytes 540676
where the time goes:
time: 296 us; the launch traced here: 295 us
  blocking collectives  101 us (34%)
  starting transfers between devices  75.3 us (25%)
  waiting for transfers between devices  69.6 us (24%)
  local copies, waits for them, and re-layouts  29.1 us (10%)
  other arithmetic  11.9 us (4%)
  matrix products  6.97 us (2%)
    all_to_all x3, blocking collectives, sent_to_all(): return lax.all_to_all(copies, axis, split_axis=0, concat_axis=0, tiled=True)  50.5 us
    all_to_all x4, waiting for transfers between devices, sum_in_two_steps(): return jnp.sum(lax.all_to_all(own, far, 0, 0, tiled=True), axis=0)  37.9 us
    all_gather x2, blocking collectives, all_in_one(): both, at, found = (lax.all_gather(jnp.concatenate(lines), axis), 0, {})  32 us
    all_to_all x3, starting transfers between devices, sent_to_all(): return lax.all_to_all(copies, axis, split_axis=0, concat_axis=0, tiled=True)  31 us
    all_to_all x4, starting transfers between devices, sum_in_two_steps(): return jnp.sum(lax.all_to_all(own, far, 0, 0, tiled=True), axis=0)  27.6 us
    all_to_all x3, waiting for transfers between devices, sent_to_all(): return lax.all_to_all(copies, axis, split_axis=0, concat_axis=0, tiled=True)  23.9 us
    all_to_all x1, blocking collectives, summed_on_arrival(): lax.all_to_all(tiles, axis, split_axis=0, concat_axis=0, tiled=True)  18.6 us
    all_to_all x4, starting transfers between devices, summed_on_arrival(): lax.all_to_all(tiles, axis, split_axis=0, concat_axis=0, tiled=True)  16.7 us
  transfers between devices with their start and end apart: 11, of which 9 were waited for; matrix products, arithmetic and copies ran while one was open for 9% of the time, Pallas kernels for 0%

commit v1 on v0

v1 whole, which is shorter than its diff:
```python
import functools

import jax
import jax.numpy as jnp
from jax import lax
from jax.experimental import pallas as pl
from jax.experimental.pallas import tpu as pltpu
from jax.sharding import PartitionSpec as P

MESH = pl.DeviceIdType.MESH
EPSILON = 1e-06
SIDE = 4
GROUP = 6
TILE = 8
ROWS = SIDE * TILE
LANES = 128
F32 = jnp.float32
BF16 = jnp.bfloat16


def dot(left, right):
    return lax.dot_general(left, right, (((1,), (0,)), ((), ())), preferred_element_type=F32)


def dot_rows(left, right):
    return lax.dot_general(left, right, (((1,), (1,)), ((), ())), preferred_element_type=F32)


def iota(shape, dim):
    return lax.broadcasted_iota(jnp.int32, shape, dim)


def far_first(count):
    return sorted(range(1, count), key=lambda k: (-min(k, count - k), k))


def split_value(value, pieces):
    parts = []
    for _ in range(pieces):
        part = value.astype(BF16)
        parts.append(part)
        value = value - part.astype(F32)
    return parts


def layer_kernel(
    ranks,
    features,
    bias,
    tokens_hbm,
    gain_a_hbm,
    gate_a_hbm,
    up_a_hbm,
    down_a_hbm,
    gain_m_hbm,
    wq_hbm,
    wk_hbm,
    wv_hbm,
    forget_hbm,
    keys_hbm,
    values_hbm,
    decay_hbm,
    wo_hbm,
    gain_b_hbm,
    gate_b_hbm,
    up_b_hbm,
    down_b_hbm,
    out_ref,
    tokens,
    gain_a,
    gate_a,
    up_a,
    down_a,
    gain_m,
    wq,
    wk,
    wv,
    forget,
    keys,
    values,
    decay,
    wo,
    gain_b,
    gate_b,
    up_b,
    down_b,
    load_sem,
    bufs_a,
    bufs_b,
    bufs_m,
):
    kv_count, tp_count = ranks
    depth = kv_count // SIDE
    kv, tp = lax.axis_index("kv"), lax.axis_index("tp")
    z, y = lax.div(kv, SIDE), lax.rem(kv, SIDE)
    chunks = gate_a.shape[1] // LANES

    def at_z(k):
        return lax.rem(z + k, depth)

    def at_y(k):
        return lax.rem(y + k, SIDE)

    def at_tp(k):
        return lax.rem(tp + k, tp_count)

    z_steps, y_steps, tp_steps = far_first(depth), far_first(SIDE), far_first(tp_count)

    barrier = pltpu.get_barrier_semaphore()
    for k in z_steps:
        pl.semaphore_signal(barrier, inc=1, device_id=(at_z(k) * SIDE + y, tp), device_id_type=MESH)
    for k in y_steps:
        pl.semaphore_signal(barrier, inc=1, device_id=(z * SIDE + at_y(k), tp), device_id_type=MESH)
    for k in tp_steps:
        pl.semaphore_signal(barrier, inc=1, device_id=(kv, at_tp(k)), device_id_type=MESH)

    block = pl.multiple_of(lax.div(kv, 2) * LANES, LANES)
    pairs = [
        (tokens_hbm, tokens),
        (gain_a_hbm, gain_a),
        (gate_a_hbm, gate_a),
        (up_a_hbm, up_a),
        (down_a_hbm, down_a),
        (decay_hbm, decay),
        (gain_m_hbm, gain_m),
        (wq_hbm, wq),
        (wk_hbm, wk),
        (wv_hbm, wv),
        (forget_hbm.at[:, pl.ds(block, LANES)], forget),
        (keys_hbm, keys),
        (values_hbm, values),
        (wo_hbm, wo),
        (gain_b_hbm, gain_b),
        (gate_b_hbm, gate_b),
        (up_b_hbm, up_b),
        (down_b_hbm, down_b),
    ]
    loads = [pltpu.make_async_copy(a, b, load_sem.at[n]) for n, (a, b) in enumerate(pairs)]
    for load in loads:
        load.start()
    waiting = list(loads)

    def loaded(count):
        for _ in range(count):
            waiting.pop(0).wait()

    sent = []

    def push(source, target, send_sem, recv_sem, device):
        copy = pltpu.make_async_remote_copy(
            src_ref=source,
            dst_ref=target,
            send_sem=send_sem,
            recv_sem=recv_sem,
            device_id=device,
            device_id_type=MESH,
        )
        copy.start()
        return copy

    def along_y(source_of, target, sems):
        send_sem, recv_sem = sems
        for k in y_steps:
            far = at_y(k)
            sent.append((None, push(
                source_of(far), target.at[y], send_sem.at[k], recv_sem.at[y], (z * SIDE + far, tp)
            )))

    def from_y(target, sems):
        for k in y_steps:
            far = at_y(k)
            slot = target.at[far]
            pltpu.make_async_copy(slot, slot, sems[1].at[far]).wait()

    def along_z(target, sems):
        send_sem, recv_sem = sems
        for k in z_steps:
            far = at_z(k)
            sent.append((None, push(
                target.at[z], target.at[z], send_sem.at[k], recv_sem.at[z], (far * SIDE + y, tp)
            )))

    def from_z(target, sems):
        for k in reversed(z_steps):
            far = at_z(k)
            slot = target.at[far]
            pltpu.make_async_copy(slot, slot, sems[1].at[far]).wait()

    def total_over_tp(partial, target, sems):
        send_sem, recv_sem = sems
        target[tp] = partial.astype(BF16)
        for k in tp_steps:
            sent.append((None, push(
                target.at[tp], target.at[tp], send_sem.at[k], recv_sem.at[tp], (kv, at_tp(k))
            )))
        for k in reversed(tp_steps):
            slot = target.at[at_tp(k)]
            pltpu.make_async_copy(slot, slot, recv_sem.at[at_tp(k)]).wait()
        total = target[0].astype(F32)
        for k in range(1, tp_count):
            total = total + target[k].astype(F32)
        return total

    sub, lane = iota((TILE, LANES), 0), iota((TILE, LANES), 1)

    def column(line, first):
        picked = jnp.where(lane == first + y * TILE + sub, jnp.broadcast_to(line, (TILE, LANES)), 0.0)
        return jnp.sum(picked, axis=1, keepdims=True)

    def squares_of(x):
        return split_value(x * x, 2)

    def owner(j):
        return lax.div(j * depth, chunks)

    def chunk_of(place):
        return lax.div(chunks * place + depth - 1, depth)

    def owns(place):
        j = chunk_of(place)
        return jnp.logical_and(j < chunks, owner(j) == place)

    def feed_forward(x, gain, gate, up, down, bufs):
        sy, ry, sz, rz, hy, rt, y_sems, zs_sems, zg_sems, h_sems, t_sems = bufs
        scaled = (x * gain[...].astype(F32)).astype(BF16)
        ones = jnp.ones((TILE, x.shape[1]), BF16)
        blank = jnp.zeros((LANES - ROWS, x.shape[1]), BF16)
        high, low = squares_of(x)
        squares = dot_rows(ones, jnp.concatenate([high, blank])) + dot_rows(
            ones, jnp.concatenate([low, blank])
        )
        for u, weight in enumerate((gate, up)):
            product = dot(scaled, weight[...])
            for g in range(SIDE):
                for j in range(chunks):
                    tile = product[g * TILE : (g + 1) * TILE, j * LANES : (j + 1) * LANES]
                    if u == 0:
                        tile = jnp.where(sub == GROUP, squares, tile)
                    sy[g, j, u] = tile.astype(BF16)
        if bufs is bufs_a:
            pl.semaphore_wait(barrier, len(z_steps) + len(y_steps) + len(tp_steps))
        along_y(lambda far: sy.at[far], ry, y_sems)
        from_y(ry, y_sems)
        total = sy[y].astype(F32)
        for k in y_steps:
            total = total + ry[at_y(k)].astype(F32)
        sz[...] = total.astype(BF16)
        for k in z_steps:
            far = at_z(k)

            @pl.when(owns(far))
            def _():
                push(
                    sz.at[chunk_of(far)],
                    rz.at[z],
                    zs_sems[0].at[k],
                    zs_sems[1].at[z],
                    (far * SIDE + y, tp),
                )

            sent.append((owns(far), (sz.at[0], zs_sems[0].at[k])))

        @pl.when(owns(z))
        def _():
            mine = chunk_of(z)
            from_z(rz, zs_sems)
            rz[z] = sz[mine]
            both = rz[0].astype(F32)
            for k in range(1, depth):
                both = both + rz[k].astype(F32)
            gate_sum, up_sum = both[0], both[1]
            factor = column(lax.rsqrt(gate_sum[GROUP : GROUP + 1] / features + EPSILON), 0)
            gate_value, up_value = factor * gate_sum, factor * up_sum
            hidden = gate_value / (1.0 + jnp.exp(-gate_value)) * up_value
            hy[y, mine] = jnp.where(sub < GROUP, hidden, 0.0).astype(BF16)
            for k in z_steps:
                push(
                    hy.at[y, mine],
                    hy.at[y, mine],
                    zg_sems[0].at[k],
                    zg_sems[1].at[mine],
                    (at_z(k) * SIDE + y, tp),
                )

        for k in z_steps:
            sent.append((owns(z), (hy.at[y, 0], zg_sems[0].at[k])))
        for k in reversed(z_steps):
            far = at_z(k)

            @pl.when(owns(far))
            def _():
                slot = hy.at[y, chunk_of(far)]
                pltpu.make_async_copy(slot, slot, zg_sems[1].at[chunk_of(far)]).wait()

        along_y(lambda far: hy.at[y], hy, h_sems)
        from_y(hy, h_sems)
        hidden = jnp.concatenate(
            [hy[:, j].astype(F32).reshape(ROWS, LANES).astype(BF16) for j in range(chunks)], axis=1
        )
        summed = total_over_tp(dot_rows(hidden, down[...]), rt, t_sems)
        return (x + 0.5 * summed).astype(BF16).astype(F32)

    def mix(x):
        (
            sq, rq, zq, zkv, qf, sa, ra, rst, za, zst, af, rt,
            q_sems, zq_sems, zkv_sems, qf_sems, a_sems, st_sems, za_sems, zst_sems, af_sems, t_sems,
        ) = bufs_m
        seqs, positions, width = keys.shape[0], decay.shape[2], x.shape[1]
        inverse = LANES ** (-0.5)

        scaled = (x * gain_m[...].astype(F32)).astype(BF16)
        high, low = squares_of(x)
        blank = jnp.zeros((ROWS, width), BF16)
        half = jnp.where(lax.rem(kv, 2) == 0, forget[:, :width].astype(F32), forget[:, width:].astype(F32))
        heads = forget.shape[0]
        r8, c8 = iota((TILE, heads), 0), iota((TILE, heads), 1)
        pick = jnp.where((r8 >= 1) & (r8 <= 2) & (c8 == 2 * tp + r8 - 1), 1.0, 0.0).astype(BF16)
        lines = dot(pick, half.astype(BF16))
        lines = jnp.where(iota((TILE, width), 0) == 0, 1.0, lines).astype(BF16)
        terms = dot_rows(lines, jnp.concatenate([high, scaled, scaled, blank]))
        extra = dot_rows(lines, jnp.concatenate([low, blank, blank, blank]))
        own_line = jnp.where(sub == lax.shift_right_logical(lane, 5), terms + jnp.where(lane < ROWS, extra, 0.0), 0.0)
        side_line = jnp.sum(own_line, axis=0, keepdims=True)
        for u, weight in enumerate((wq, wk, wv)):
            product = dot(scaled, weight[...])
            for g in range(SIDE):
                for h in range(2):
                    tile = product[g * TILE : (g + 1) * TILE, h * LANES : (h + 1) * LANES]
                    if u == 0 and h == 0:
                        tile = jnp.where(sub == GROUP, jnp.broadcast_to(side_line, (TILE, LANES)), tile)
                    sq[g, 2 * u + h] = tile.astype(BF16)
        along_y(lambda far: sq.at[far], rq, q_sems)
        from_y(rq, q_sems)
        total = sq[y].astype(F32)
        for k in y_steps:
            total = total + rq[at_y(k)].astype(F32)
        total = total.astype(BF16)
        zq[z] = total[:2]
        along_z(zq, zq_sems)
        zkv[z] = total[2:]
        along_z(zkv, zkv_sems)

        from_z(zq, zq_sems)
        both = zq[0].astype(F32)
        for k in range(1, depth):
            both = both + zq[k].astype(F32)
        line = both[0][GROUP : GROUP + 1]
        factor = column(lax.rsqrt(line / features + EPSILON), 0)
        query = [jnp.where(sub < GROUP, factor * both[h], 0.0).astype(BF16) for h in range(2)]
        for h in range(2):
            qf[y, h] = query[h]
        along_y(lambda far: qf.at[y], qf, qf_sems)
        log_gate = []
        for h in range(2):
            gate = factor * column(line, ROWS * (h + 1)) + bias[2 * tp + h]
            log_gate.append(jnp.minimum(gate, 0.0) - jnp.log(1.0 + jnp.exp(-jnp.abs(gate))))

        from_y(qf, qf_sems)
        lane2 = iota((TILE, 2 * positions), 1)
        even = lax.rem(lane2, 2) == 0
        sub2 = iota((TILE, 2 * positions), 0)
        stats = jnp.zeros((1, LANES), F32)
        for g in range(SIDE):
            pair = jnp.concatenate([qf[g, 0].astype(F32), qf[g, 1].astype(F32)]).astype(BF16)
            scores = jnp.zeros((TILE, 2 * positions), F32)
            for i in range(GROUP):
                found = dot_rows(pair, keys[g * GROUP + i])
                found = jnp.where(even, found[:TILE], found[TILE:])
                scores = jnp.where(sub2 == i, found, scores)
            scores = scores * inverse + spread[g * TILE : (g + 1) * TILE]
            tops = [
                jnp.max(jnp.where(even if h == 0 else ~even, scores, -jnp.inf), axis=1, keepdims=True)
                for h in range(2)
            ]
            weights = jnp.exp(scores - jnp.where(even, tops[0], tops[1])).astype(BF16).astype(F32)
            parts = [jnp.where(even, weights, 0.0), jnp.where(even, 0.0, weights)]
            sums = [jnp.sum(part, axis=1, keepdims=True) for part in parts]
            both_parts = jnp.concatenate(parts).astype(BF16)
            mixed = [jnp.zeros((TILE, LANES), F32) for _ in range(2)]
            for i in range(GROUP):
                found = dot(both_parts, values[g * GROUP + i])
                for h in range(2):
                    mixed[h] = jnp.where(sub == i, found[h * TILE : (h + 1) * TILE], mixed[h])
            for h in range(2):
                sa[g, h] = (mixed[h] / sums[h]).astype(BF16)
                level = tops[h] + jnp.log(sums[h])
                stats = stats + jnp.sum(
                    jnp.where(lane == ROWS * h + g * TILE + sub, level, 0.0), axis=0, keepdims=True
                )
        rst[y] = stats
        along_y(lambda far: sa.at[far], ra, a_sems)
        along_y(lambda far: rst.at[y], rst, st_sems)
        from_y(rst, st_sems)
        from_y(ra, a_sems)

        def merged(levels, parts):
            top = functools.reduce(jnp.maximum, levels)
            shares = [jnp.exp(level - top) for level in levels]
            whole = sum(shares[1:], shares[0])
            value = sum((a * b for a, b in zip(shares[1:], parts[1:])), shares[0] * parts[0])
            return value / whole, top + jnp.log(whole)

        spots = [y] + [at_y(k) for k in y_steps]
        stats = jnp.zeros((1, LANES), F32)
        for h in range(2):
            levels = [column(rst[spot], ROWS * h) for spot in spots]
            parts = [sa[y, h].astype(F32)] + [ra[spot, h].astype(F32) for spot in spots[1:]]
            value, level = merged(levels, parts)
            za[z, h] = value.astype(BF16)
            stats = stats + jnp.sum(
                jnp.where(lane == ROWS * h + y * TILE + sub, level, 0.0), axis=0, keepdims=True
            )
        zst[z] = stats
        along_z(zst, zst_sems)
        along_z(za, za_sems)

        from_z(zkv, zkv_sems)
        both = zkv[0].astype(F32)
        for k in range(1, depth):
            both = both + zkv[k].astype(F32)
        fresh = [jnp.where(sub < GROUP, factor * both[u], 0.0).astype(BF16).astype(F32) for u in range(4)]
        own_level = [
            jnp.sum(query[h].astype(F32) * fresh[h], axis=1, keepdims=True) * inverse for h in range(2)
        ]
        from_z(zst, zst_sems)
        from_z(za, za_sems)
        for h in range(2):
            levels = [column(zst[k], ROWS * h) + log_gate[h] for k in range(depth)] + [own_level[h]]
            parts = [za[k, h].astype(F32) for k in range(depth)] + [fresh[2 + h]]
            af[y, h] = merged(levels, parts)[0].astype(BF16)
        along_y(lambda far: af.at[y], af, af_sems)
        from_y(af, af_sems)
        attended = jnp.concatenate(
            [af[:, h].astype(F32).reshape(ROWS, LANES).astype(BF16) for h in range(2)], axis=1
        )
        summed = total_over_tp(dot_rows(attended, wo[...]), rt, t_sems)
        return (x + summed).astype(BF16).astype(F32)

    seqs = tokens.shape[0]
    to_rows = iota((ROWS, seqs), 0)
    seat = lax.shift_right_logical(to_rows, 3) * GROUP + (to_rows & 7)
    place = jnp.where(((to_rows & 7) < GROUP) & (seat == iota((ROWS, seqs), 1)), 1.0, 0.0).astype(BF16)

    loaded(4)
    x = dot(place, tokens[...])
    loaded(1)
    loaded(1)
    positions = decay.shape[2]
    spread = jnp.zeros((ROWS, 2 * positions), F32)
    pieces = [split_value(decay[:, h, :], 3) for h in range(2)]
    for n in range(3):
        woven = jnp.zeros((seqs, 2 * positions), F32)
        for h in range(2):
            weave = jnp.where(
                iota((positions, 2 * positions), 1) == 2 * iota((positions, 2 * positions), 0) + h, 1.0, 0.0
            ).astype(BF16)
            woven = woven + dot(pieces[h][n], weave)
        spread = spread + dot(place, woven.astype(BF16))

    first = feed_forward(x, gain_a, gate_a, up_a, down_a, bufs_a)

    loaded(8)
    second = mix(first)
    loaded(4)
    last = feed_forward(second, gain_b, gate_b, up_b, down_b, bufs_b)

    back = iota((seqs, ROWS), 1)
    seat = lax.shift_right_logical(back, 3) * GROUP + (back & 7)
    lift = jnp.where(((back & 7) < GROUP) & (seat == iota((seqs, ROWS), 0)), 1.0, 0.0).astype(BF16)
    out_ref[...] = dot(lift, last.astype(BF16)).astype(BF16)

    for condition, copy in sent:
        if condition is None:
            copy.wait_send()
        else:
            ref, sem = copy

            @pl.when(condition)
            def _():
                pltpu.make_async_copy(ref, ref, sem).wait()


def on_device(
    ranks,
    tokens,
    gain_first,
    gate_first,
    up_first,
    down_first,
    gain_mixer,
    query_weight,
    key_weight,
    value_weight,
    forget_weight,
    forget_bias,
    key_cache,
    value_cache,
    forget_sum,
    out_weight,
    gain_second,
    gate_second,
    up_second,
    down_second,
):
    kv_count, tp_count = ranks
    depth = kv_count // SIDE
    seqs, length = key_cache.shape[:2]
    chunks = gate_first.shape[1] // LANES
    width = tokens.shape[1]
    dma = pltpu.SemaphoreType.DMA

    def flat(cache):
        return cache.reshape(seqs, 2 * length, LANES)

    operands = [
        tokens,
        gain_first.reshape(1, -1),
        gate_first,
        up_first,
        down_first.T,
        gain_mixer.reshape(1, -1),
        query_weight,
        key_weight,
        value_weight,
        forget_weight.T,
        flat(key_cache),
        flat(value_cache),
        forget_sum,
        out_weight.T,
        gain_second.reshape(1, -1),
        gate_second,
        up_second,
        down_second.T,
    ]
    held = [pltpu.VMEM(a.shape, a.dtype) for a in operands]
    held[9] = pltpu.VMEM((forget_weight.shape[1], LANES), BF16)

    def tiles(*dims):
        return pltpu.VMEM((*dims, TILE, LANES), BF16)

    def pair(count, other=None):
        return (dma((count,)), dma((other or count,)))

    def bufs():
        return (
            tiles(SIDE, chunks, 2),
            tiles(SIDE, chunks, 2),
            tiles(chunks, 2),
            tiles(depth, 2),
            tiles(SIDE, chunks),
            pltpu.VMEM((tp_count, ROWS, width), BF16),
            pair(SIDE),
            pair(depth),
            pair(depth, chunks),
            pair(SIDE),
            pair(tp_count),
        )

    mix_bufs = (
        tiles(SIDE, 6),
        tiles(SIDE, 6),
        tiles(depth, 2),
        tiles(depth, 4),
        tiles(SIDE, 2),
        tiles(SIDE, 2),
        tiles(SIDE, 2),
        pltpu.VMEM((SIDE, 1, LANES), F32),
        tiles(depth, 2),
        pltpu.VMEM((depth, 1, LANES), F32),
        tiles(SIDE, 2),
        pltpu.VMEM((tp_count, ROWS, width), BF16),
        pair(SIDE),
        pair(depth),
        pair(depth),
        pair(SIDE),
        pair(SIDE),
        pair(SIDE),
        pair(depth),
        pair(depth),
        pair(SIDE),
        pair(tp_count),
    )
    return pl.pallas_call(
        functools.partial(layer_kernel, ranks, width * kv_count),
        out_shape=jax.ShapeDtypeStruct(tokens.shape, BF16),
        in_specs=[pl.BlockSpec(memory_space=pltpu.SMEM)]
        + [pl.BlockSpec(memory_space=pltpu.HBM)] * len(operands),
        out_specs=pl.BlockSpec(memory_space=pltpu.VMEM),
        scratch_shapes=held + [dma((len(operands),)), bufs(), bufs(), mix_bufs],
        compiler_params=pltpu.CompilerParams(
            collective_id=0, has_side_effects=True, vmem_limit_bytes=48 * 1024 * 1024
        ),
        name="layer",
    )(forget_bias, *operands)


def solution(mesh):
    ranks = (mesh.shape["kv"], mesh.shape["tp"])
    kv, tp = "kv", "tp"
    in_specs = (
        P(None, kv),
        P(kv),
        P(kv, tp),
        P(kv, tp),
        P(tp, kv),
        P(kv),
        P(kv, tp),
        P(kv, tp),
        P(kv, tp),
        P(),
        P(),
        P(None, kv, tp, None),
        P(None, kv, tp, None),
        P(None, tp, kv),
        P(tp, kv),
        P(kv),
        P(kv, tp),
        P(kv, tp),
        P(tp, kv),
    )
    return jax.shard_map(
        functools.partial(on_device, ranks),
        mesh=mesh,
        in_specs=in_specs,
        out_specs=P(None, kv),
        check_vma=False,
    )
```

time: 296 us -> 125 us (0.42)
  Pallas kernels: 0 us -> 108 us
  blocking collectives: 101 us -> 0 us
  starting transfers between devices: 75.3 us -> 0 us
  waiting for transfers between devices: 69.6 us -> 0 us
  local copies, waits for them, and re-layouts: 29.1 us -> 16.9 us
  other arithmetic: 11.9 us -> 0 us
  matrix products: 6.97 us -> 0 us
    pallas_call x0 -> x1, Pallas kernels: none -> 108 us  [on_device(): pl.pallas_call(functools.partial(layer_kernel, ranks, width * kv_count),...]
    all_to_all x11 -> x0, starting transfers between devices: 75.3 us -> none  [the longest x3 31 us: sent_to_all(): return lax.all_to_all(copies, axis, split_axis=0, concat_axis=0, tiled=True)]
    all_to_all x11 -> x0, waiting for transfers between devices: 69.6 us -> none  [the longest x4 37.9 us: sum_in_two_steps(): return jnp.sum(lax.all_to_all(own, far, 0, 0, tiled=True), axis=0)]
    all_to_all x4 -> x0, blocking collectives: 69.1 us -> none  [the longest x3 50.5 us: sent_to_all(): return lax.all_to_all(copies, axis, split_axis=0, concat_axis=0, tiled=True)]
    all_gather x2 -> x0, blocking collectives: 32 us -> none  [all_in_one(): both, at, found = (lax.all_gather(jnp.concatenate(lines), axis), 0, {})]
    dot_general x13 -> x0, matrix products: 6.97 us -> none  [the longest x1 1.92 us: mix_tokens(): jnp.einsum('bhcs,bcshd->bhcd', weights, value_cache.reshape(seq_count, bl...]
    all_to_all x7 -> x0, other arithmetic: 6.19 us -> none  [the longest x4 4.26 us: summed_on_arrival(): lax.all_to_all(tiles, axis, split_axis=0, concat_axis=0, tiled=True)]
    transpose x4 -> x0, local copies, waits for them, and re-layouts: 4.14 us -> none  [the longest x2 3.99 us: split_up(): return jnp.moveaxis(tiles, dim, 0)]
  transfers between devices with their start and end apart: 11 -> 0, of which waited for: 9 -> 0; matrix products, arithmetic and copies ran while one was open for 9% -> 0% of each run, Pallas kernels for 0% -> 0%
where the time goes in v1:
time: 125 us
  Pallas kernels  108 us (86%)
  local copies, waits for them, and re-layouts  16.9 us (14%)
    pallas_call x1, Pallas kernels, on_device(): pl.pallas_call(functools.partial(layer_kernel, ranks, width * kv_count),...  108 us
    unnamed x39, local copies, waits for them, and re-layouts  16.9 us

profile of v1, /device:TPU:1, one launch (start us, length us, event | category | flops | bytes accessed | tf_op | source)
XLA Modules:
  0.0 124.7 jit_solution(4251875156110045623)
XLA Ops:
  0.0 0.0 copy-start
  0.0 1.4 %copy-done = bf16[24,128,2,128]{3,2,1,0:T(2,128)(2,1)S(1)} copy-done((bf16[24,128,2,128]{3,2,1,0:T(2,128)(2,1)S(1)}, bf16[24,128,2,128]{3,2,1,0:T(2,128)(2,1)}, u32[]{:S(2)}) %copy-start) | copy-done | bytes 1572888
  1.4 0.0 copy-start.1
  1.4 1.4 %copy-done.1 = bf16[24,128,2,128]{3,2,1,0:T(2,128)(2,1)S(1)} copy-done((bf16[24,128,2,128]{3,2,1,0:T(2,128)(2,1)S(1)}, bf16[24,128,2,128]{3,2,1,0:T(2,128)(2,1)}, u32[]{:S(2)}) %copy-start.1) | copy-done | bytes 1572888
  2.8 0.0 copy-start.2
  2.8 0.9 copy-done.2
  3.7 0.0 copy-start.3
  3.7 0.9 copy-done.3
  4.7 0.0 copy-start.4
  4.7 0.9 copy-done.4
  5.6 0.0 copy-start.5
  5.6 0.9 copy-done.5
  6.5 0.0 copy-start.6
  6.5 0.9 copy-done.6
  7.4 0.0 copy-start.7
  7.4 0.9 copy-done.7
  8.3 0.0 copy-start.8
  8.4 0.9 copy-done.8
  9.3 0.0 copy-start.9
  9.3 0.8 copy-done.9
  10.0 0.0 copy-start.10
  10.0 0.8 copy-done.10
  10.8 0.0 copy-start.11
  10.8 0.8 copy-done.11
  11.5 0.0 copy-start.12
  11.5 0.8 copy-done.12
  12.3 0.0 copy-start.13
  12.3 0.7 copy-done.13
  13.0 0.0 copy-start.14
  13.0 0.7 copy-done.14
  13.7 0.0 copy-start.15
  13.7 0.7 copy-done.15
  14.4 0.0 copy-start.16
  14.4 0.7 copy-done.16
  15.0 0.0 copy-start.17
  15.0 0.7 copy-done.17
  15.7 0.0 copy-start.18
  15.7 0.7 copy-done.18
  16.3 107.8 %layer.1 = bf16[24,64]{1,0:T(8,128)(2,1)S(1)} custom-call(f32[16]{0:T(128)S(1)} %copy-done.15, bf16[24,64]{1,0:T(8,128)(2,1)S(1)} %copy-done.14, bf16[1,64]{1,0:T(2,128)(2,1)S(1)} %bitcast.15, bf16[64,1408]{1,0:T(8,128)(2,1)S(1)} %copy-done.2, bf16[64,1408]{1,0:T(8,128)(2,1)S(1)} %copy-done.3, bf16[64,1408]{1,0:T(8,128)(2,1)S(1)} %bitcast.11, ...), custom_call_target="tpu_custom_call" | custom-call | tf_op jit(solution)/shard_map/layer/pallas_call | solution.py:583
  124.1 0.6 copy.21
Async XLA Ops:
  0.0 1.4 %copy-start = (bf16[24,128,2,128]{3,2,1,0:T(2,128)(2,1)S(1)}, bf16[24,128,2,128]{3,2,1,0:T(2,128)(2,1)}, u32[]{:S(2)}) copy-start(bf16[24,128,2,128]{3,2,1,0:T(2,128)(2,1)} %param.30) | copy-start | bytes 4718596
  1.4 1.4 %copy-start.1 = (bf16[24,128,2,128]{3,2,1,0:T(2,128)(2,1)S(1)}, bf16[24,128,2,128]{3,2,1,0:T(2,128)(2,1)}, u32[]{:S(2)}) copy-start(bf16[24,128,2,128]{3,2,1,0:T(2,128)(2,1)} %param.31) | copy-start | bytes 4718596
  2.8 0.9 copy-start.2
  3.7 0.9 copy-start.3
  4.7 0.9 copy-start.4
  5.6 0.9 copy-start.5
  6.5 0.9 copy-start.6
  7.4 0.9 copy-start.7
  8.3 0.9 copy-start.8
  9.3 0.8 copy-start.9
  10.0 0.8 copy-start.10
  10.8 0.8 copy-start.11
  11.5 0.8 copy-start.12
  12.3 0.7 copy-start.13
  13.0 0.7 copy-start.14
  13.7 0.7 copy-start.15
  14.4 0.7 copy-start.16
  15.0 0.7 copy-start.17
  15.7 0.7 copy-start.18

commit v2 on v1

v2 whole, which is shorter than its diff:
```python
import functools

import jax
import jax.numpy as jnp
from jax import lax
from jax.experimental import pallas as pl
from jax.experimental.pallas import tpu as pltpu
from jax.sharding import PartitionSpec as P

MESH = pl.DeviceIdType.MESH
EPSILON = 1e-06
SIDE = 4
GROUP = 6
TILE = 8
ROWS = SIDE * TILE
LANES = 128
F32 = jnp.float32
BF16 = jnp.bfloat16


def dot(left, right):
    return lax.dot_general(left, right, (((1,), (0,)), ((), ())), preferred_element_type=F32)


def dot_rows(left, right):
    return lax.dot_general(left, right, (((1,), (1,)), ((), ())), preferred_element_type=F32)


def iota(shape, dim):
    return lax.broadcasted_iota(jnp.int32, shape, dim)


def far_first(count):
    return sorted(range(1, count), key=lambda k: (-min(k, count - k), k))


def split_value(value, pieces):
    parts = []
    for _ in range(pieces):
        part = value.astype(BF16)
        parts.append(part)
        value = value - part.astype(F32)
    return parts


def layer_kernel(
    ranks,
    features,
    bias,
    tokens_hbm,
    gain_a_hbm,
    gate_a_hbm,
    up_a_hbm,
    down_a_hbm,
    gain_m_hbm,
    wq_hbm,
    wk_hbm,
    wv_hbm,
    forget_hbm,
    keys_hbm,
    values_hbm,
    decay_hbm,
    wo_hbm,
    gain_b_hbm,
    gate_b_hbm,
    up_b_hbm,
    down_b_hbm,
    out_ref,
    tokens,
    gain_a,
    gate_a,
    up_a,
    gain_m,
    gain_b,
    forget,
    keys,
    values,
    decay,
    down_a,
    gates_b,
    down_b,
    w_all,
    wo_all,
    down_a_all,
    gates_b_all,
    down_b_all,
    load_sem,
    tiles_y,
    tiles_all,
    sy,
    ry,
    ff_a,
    ff_b,
    mix_bufs,
    t_one,
    t_two,
    t_three,
    first_all,
    tok_sems,
    y_sems,
    down_a_sems,
    w_sems,
    wo_sems,
    gates_b_sems,
    down_b_sems,
    first_sems,
):
    kv_count, tp_count = ranks
    depth = kv_count // SIDE
    kv, tp = lax.axis_index("kv"), lax.axis_index("tp")
    z, y = lax.div(kv, SIDE), lax.rem(kv, SIDE)
    chunks = gate_a.shape[1] // LANES
    share = down_a.shape[0] // SIDE
    pieces = share * SIDE
    width = tokens.shape[1]
    slab = SIDE * width
    seqs = tokens.shape[0]
    positions = decay.shape[2]

    def at_z(k):
        return lax.rem(z + k, depth)

    def at_y(k):
        return lax.rem(y + k, SIDE)

    def at_tp(k):
        return lax.rem(tp + k, tp_count)

    z_steps, y_steps = far_first(depth), far_first(SIDE)
    plane = sorted(
        [(a, b) for a in range(SIDE) for b in range(tp_count) if a or b],
        key=lambda s: (-min(s[0], SIDE - s[0]) - min(s[1], tp_count - s[1]) / 2, s),
    )

    barrier = pltpu.get_barrier_semaphore()
    for k in z_steps:
        pl.semaphore_signal(barrier, inc=1, device_id=(at_z(k) * SIDE + y, tp), device_id_type=MESH)
    for a, b in plane:
        pl.semaphore_signal(barrier, inc=1, device_id=(z * SIDE + at_y(a), at_tp(b)), device_id_type=MESH)

    def columns(ref, j):
        return ref.at[:, pl.ds(j * LANES, LANES)]

    groups = {
        "tokens": [(tokens_hbm, tokens), (gain_a_hbm, gain_a), (gain_m_hbm, gain_m), (gain_b_hbm, gain_b)],
        "gate_a": [(gate_a_hbm, gate_a)],
        "up_a": [(up_a_hbm, up_a)],
        "down_a": [(columns(down_a_hbm, j), down_a.at[j]) for j in range(chunks)],
        "decay": [(decay_hbm, decay)],
        "w": [(wq_hbm, w_all.at[0, y]), (wk_hbm, w_all.at[1, y]), (wv_hbm, w_all.at[2, y])],
        "wo": [(wo_hbm, wo_all.at[y])],
        "forget": [(forget_hbm.at[:, pl.ds(pl.multiple_of(z * slab, slab), slab)], forget)],
        "keys": [(keys_hbm, keys)],
        "values": [(values_hbm, values)],
        "gates_b": [(columns(gate_b_hbm, j), gates_b.at[j, 0]) for j in range(chunks)]
        + [(columns(up_b_hbm, j), gates_b.at[j, 1]) for j in range(chunks)],
        "down_b": [(columns(down_b_hbm, j), down_b.at[j]) for j in range(chunks)],
    }
    loads, count = {}, 0
    for name, copies in groups.items():
        loads[name] = []
        for a, b in copies:
            load = pltpu.make_async_copy(a, b, load_sem.at[count])
            load.start()
            loads[name].append(load)
            count += 1

    def loaded(*names):
        for name in names:
            for load in loads.pop(name):
                load.wait()

    sent = []

    def push(source, target, send_sem, recv_sem, device):
        copy = pltpu.make_async_remote_copy(
            src_ref=source,
            dst_ref=target,
            send_sem=send_sem,
            recv_sem=recv_sem,
            device_id=device,
            device_id_type=MESH,
        )
        copy.start()
        return copy

    def await_slot(slot, sem):
        pltpu.make_async_copy(slot, slot, sem).wait()

    def along_y(source_of, target_of, sems):
        for k in y_steps:
            far = at_y(k)
            sent.append((None, push(
                source_of(far), target_of(y), sems[0].at[k], sems[1].at[y], (z * SIDE + far, tp)
            )))

    def from_y(target_of, sems):
        for k in y_steps:
            far = at_y(k)
            await_slot(target_of(far), sems[1].at[far])

    def along_z(target, sems):
        for k in z_steps:
            far = at_z(k)
            sent.append((None, push(
                target.at[z], target.at[z], sems[0].at[k], sems[1].at[z], (far * SIDE + y, tp)
            )))

    def from_z(target, sems):
        for k in reversed(z_steps):
            far = at_z(k)
            await_slot(target.at[far], sems[1].at[far])

    def over_plane(source_of, target, sems):
        for n, (a, b) in enumerate(plane):
            far = at_y(a)
            sent.append((None, push(
                source_of(far), target.at[y, tp], sems[0].at[n], sems[1].at[y, tp], (z * SIDE + far, at_tp(b))
            )))

    def from_plane(target, sems):
        for a, b in reversed(plane):
            await_slot(target.at[at_y(a), at_tp(b)], sems[1].at[at_y(a), at_tp(b)])

    sub, lane = iota((TILE, LANES), 0), iota((TILE, LANES), 1)

    def column(line, first):
        picked = jnp.where(lane == first + sub, jnp.broadcast_to(line, (TILE, LANES)), 0.0)
        return jnp.sum(picked, axis=1, keepdims=True)

    def as_line(values, first):
        shape = (values.shape[0], LANES)
        spread_out = jnp.where(iota(shape, 1) == first + iota(shape, 0), values, 0.0)
        return jnp.sum(spread_out, axis=0, keepdims=True)

    def row_sum(x):
        return jnp.sum(x, axis=1, keepdims=True)

    def owner(p):
        return lax.div(p * depth, pieces)

    def piece_of(place):
        return lax.div(pieces * place + depth - 1, depth)

    def owns(place):
        p = piece_of(place)
        return jnp.logical_and(p < pieces, owner(p) == place)

    def send_pieces(bufs, n):
        sz, rz, hz, rs_sems, ag_sems = bufs
        for k in z_steps:
            far = at_z(k)
            p = piece_of(far)

            @pl.when(jnp.logical_and(owns(far), lax.div(p, SIDE) == n))
            def _():
                push(sz.at[p], rz.at[z], rs_sems[0].at[k], rs_sems[1].at[z], (far * SIDE + y, tp))

    def hidden_units(bufs):
        sz, rz, hz, rs_sems, ag_sems = bufs
        for k in z_steps:
            sent.append((owns(at_z(k)), (sz.at[0], rs_sems[0].at[k])))

        @pl.when(owns(z))
        def _():
            mine = piece_of(z)
            with jax.named_scope("z_reduce"):
                from_z(rz, rs_sems)
            rz[z] = sz[mine]
            both = rz[0].astype(F32)
            for k in range(1, depth):
                both = both + rz[k].astype(F32)
            gate_sum, up_sum = both[0], both[1]
            factor = lax.rsqrt(gate_sum[GROUP : GROUP + 1] / features + EPSILON)
            factor = column(factor, lax.rem(mine, SIDE) * TILE)
            gate_value, up_value = factor * gate_sum, factor * up_sum
            hidden = gate_value / (1.0 + jnp.exp(-gate_value)) * up_value
            hz[mine] = jnp.where(sub < GROUP, hidden, 0.0).astype(BF16)
            for k in z_steps:
                push(hz.at[mine], hz.at[mine], ag_sems[0].at[k], ag_sems[1].at[mine], (at_z(k) * SIDE + y, tp))

        for k in z_steps:
            sent.append((owns(z), (hz.at[0], ag_sems[0].at[k])))
        with jax.named_scope("z_gather"):
            for k in reversed(z_steps):
                far = at_z(k)

                @pl.when(owns(far))
                def _():
                    await_slot(hz.at[piece_of(far)], ag_sems[1].at[piece_of(far)])

        return [
            hz[n * SIDE : (n + 1) * SIDE].astype(F32).reshape(ROWS, LANES).astype(BF16) for n in range(share)
        ]

    to_rows = iota((ROWS, seqs), 0)
    seat = lax.shift_right_logical(to_rows, 3) * GROUP + (to_rows & 7)
    place = jnp.where(((to_rows & 7) < GROUP) & (seat == iota((ROWS, seqs), 1)), 1.0, 0.0).astype(BF16)

    loaded("tokens")
    x = dot(place, tokens[...])
    gain_rows = [jnp.broadcast_to(g[...].astype(F32), (ROWS, width)) for g in (gain_m, gain_b)]
    row_in_tile = iota((ROWS, width), 0) & 7
    with_gains = jnp.where(row_in_tile == GROUP, gain_rows[0], jnp.where(row_in_tile == GROUP + 1, gain_rows[1], x))
    for g in range(SIDE):
        tiles_y[g] = with_gains[g * TILE : (g + 1) * TILE].astype(BF16)
    tiles_all[y] = tiles_y[y]

    scaled = (x * gain_a[...].astype(F32)).astype(BF16)
    squares = jnp.broadcast_to(as_line(row_sum(x * x), 0), (TILE, LANES))
    loaded("gate_a", "up_a")
    for u, weight in enumerate((gate_a, up_a)):
        product = dot(scaled, weight[...])
        for j in range(chunks):
            for g in range(SIDE):
                tile = product[g * TILE : (g + 1) * TILE, j * LANES : (j + 1) * LANES]
                if u == 0:
                    tile = jnp.where(sub == GROUP, squares, tile)
                sy[j // share, (j % share) * SIDE + g, u] = tile.astype(BF16)
    for j in range(chunks, pieces):
        for g in range(SIDE):
            for u in range(2):
                sy[j // share, (j % share) * SIDE + g, u] = jnp.zeros((TILE, LANES), BF16)
        down_a[j] = jnp.zeros((width, LANES), BF16)
        for u in range(2):
            gates_b[j, u] = jnp.zeros((width, LANES), BF16)
        down_b[j] = jnp.zeros((width, LANES), BF16)

    with jax.named_scope("barrier"):
        pl.semaphore_wait(barrier, len(z_steps) + len(plane))

    def portion(ref, which, n):
        return ref.at[which, pl.ds(n * SIDE, SIDE)]

    for n in range(share):
        along_y(lambda far: portion(sy, far, n), lambda near: portion(ry, near, n), [s.at[n] for s in y_sems])
    along_y(lambda far: tiles_y.at[far], lambda near: tiles_all.at[near], tok_sems)
    loaded("down_a")
    along_y(lambda far: down_a.at[pl.ds(far * share, share)], lambda near: down_a_all.at[:, near], down_a_sems)
    down_a_all[:, y] = down_a[pl.ds(y * share, share)]
    loaded("w")
    for u in range(3):
        along_y(lambda far: w_all.at[u, y], lambda near: w_all.at[u, near], [s.at[u] for s in w_sems])
    loaded("wo")
    along_y(lambda far: wo_all.at[y], lambda near: wo_all.at[near], wo_sems)

    sz = ff_a[0]
    for n in range(share):
        with jax.named_scope("y_reduce"):
            from_y(lambda near: portion(ry, near, n), [s.at[n] for s in y_sems])
        rows = pl.ds(n * SIDE, SIDE)
        total = sy[y, rows].astype(F32)
        for k in y_steps:
            total = total + ry[at_y(k), rows].astype(F32)
        sz[rows] = total.astype(BF16)
        send_pieces(ff_a, n)

    loaded("decay")
    spread = jnp.zeros((ROWS, 2 * positions), F32)
    thirds = [split_value(decay[:, h, :], 3) for h in range(2)]
    for n in range(3):
        woven = jnp.zeros((seqs, 2 * positions), F32)
        for h in range(2):
            weave = jnp.where(
                iota((positions, 2 * positions), 1) == 2 * iota((positions, 2 * positions), 0) + h, 1.0, 0.0
            ).astype(BF16)
            woven = woven + dot(thirds[h][n], weave)
        spread = spread + dot(place, woven.astype(BF16))
    from_y(lambda near: tiles_all.at[near], tok_sems)
    own_rows = jnp.zeros((TILE, slab), F32)
    for g in range(SIDE):
        lift = jnp.where(iota((width, slab), 1) == iota((width, slab), 0) + g * width, 1.0, 0.0).astype(BF16)
        own_rows = own_rows + dot(tiles_all[g], lift)
    gain_m_slab, gain_b_slab = own_rows[GROUP : GROUP + 1], own_rows[GROUP + 1 : GROUP + 2]
    wide = iota((TILE, slab), 0) < GROUP
    own_rows = jnp.where(wide, own_rows, 0.0)

    hidden = hidden_units(ff_a)
    from_y(lambda near: down_a_all.at[:, near], down_a_sems)
    partial = jnp.zeros((ROWS, slab), F32)
    for n in range(share):
        partial = partial + dot_rows(hidden[n], down_a_all[n].reshape(slab, LANES))
    send_one, got_one, one_sems = t_one
    for g in range(SIDE):
        send_one[g] = partial[g * TILE : (g + 1) * TILE].astype(BF16)
    got_one[y, tp] = send_one[y]
    over_plane(lambda far: send_one.at[far], got_one, one_sems)
    loaded("gates_b", "down_b")
    with jax.named_scope("plane_one"):
        from_plane(got_one, one_sems)

    def added(ref):
        total = ref[0].astype(F32)
        for k in range(1, tp_count):
            total = total + ref[k].astype(F32)
        return total

    summed = sum((added(got_one.at[g]) for g in range(1, SIDE)), added(got_one.at[0]))
    first_rows = (own_rows + 0.5 * summed).astype(BF16)
    first_all[y] = first_rows

    (
        zq, zkv, qf, sa, ra, rst, za, zst,
        zq_sems, zkv_sems, qf_sems, a_sems, st_sems, za_sems, zst_sems,
    ) = mix_bufs
    inverse = LANES ** (-0.5)
    x = first_rows.astype(F32)
    scaled = (x * gain_m_slab).astype(BF16)
    loaded("forget")
    heads = forget.shape[0]
    r8, c8 = iota((TILE, heads), 0), iota((TILE, heads), 1)
    pick = jnp.where((r8 < 2) & (c8 == 2 * tp + r8), 1.0, 0.0).astype(BF16)
    lines = dot(pick, forget[...])
    side_line = as_line(row_sum(x * x), 0)
    for h in range(2):
        side_line = side_line + as_line(row_sum(scaled.astype(F32) * lines[h : h + 1]), ROWS * (h + 1))
    side_line = jnp.broadcast_to(side_line, (TILE, LANES))
    with jax.named_scope("w_wait"):
        for u in range(3):
            from_y(lambda near: w_all.at[u, near], [s.at[u] for s in w_sems])
    product = [dot(scaled, w_all[u].reshape(slab, 2 * LANES)) for u in range(3)]
    for h in range(2):
        tile = product[0][:, h * LANES : (h + 1) * LANES]
        zq[z, h] = (jnp.where(sub == GROUP, side_line, tile) if h == 0 else tile).astype(BF16)
    along_z(zq, zq_sems)
    for u in range(2):
        for h in range(2):
            zkv[z, 2 * u + h] = product[1 + u][:, h * LANES : (h + 1) * LANES].astype(BF16)
    along_z(zkv, zkv_sems)
    along_y(lambda far: first_all.at[y], lambda near: first_all.at[near], first_sems)
    along_y(
        lambda far: gates_b.at[pl.ds(far * share, share)], lambda near: gates_b_all.at[:, :, near], gates_b_sems
    )
    along_y(lambda far: down_b.at[pl.ds(far * share, share)], lambda near: down_b_all.at[:, near], down_b_sems)
    gates_b_all[:, :, y] = gates_b[pl.ds(y * share, share)]
    down_b_all[:, y] = down_b[pl.ds(y * share, share)]

    with jax.named_scope("z_query"):
        from_z(zq, zq_sems)
    both = zq[0].astype(F32)
    for k in range(1, depth):
        both = both + zq[k].astype(F32)
    line = both[0][GROUP : GROUP + 1]
    factor = column(lax.rsqrt(line / features + EPSILON), 0)
    query = [jnp.where(sub < GROUP, factor * both[h], 0.0).astype(BF16) for h in range(2)]
    for h in range(2):
        qf[y, h] = query[h]
    along_y(lambda far: qf.at[y], lambda near: qf.at[near], qf_sems)
    log_gate = []
    for h in range(2):
        gate = factor * column(line, ROWS * (h + 1)) + bias[2 * tp + h]
        log_gate.append(jnp.minimum(gate, 0.0) - jnp.log(1.0 + jnp.exp(-jnp.abs(gate))))
    loaded("keys", "values")

    with jax.named_scope("y_query"):
        from_y(lambda near: qf.at[near], qf_sems)
    lane2, sub2 = iota((TILE, 2 * positions), 1), iota((TILE, 2 * positions), 0)
    even = lax.rem(lane2, 2) == 0
    stats = jnp.zeros((1, LANES), F32)
    for g in range(SIDE):
        pair = jnp.concatenate([qf[g, 0].astype(F32), qf[g, 1].astype(F32)]).astype(BF16)
        scores = jnp.zeros((TILE, 2 * positions), F32)
        for i in range(GROUP):
            found = dot_rows(pair, keys[g * GROUP + i])
            found = jnp.where(even, found[:TILE], found[TILE:])
            scores = jnp.where(sub2 == i, found, scores)
        scores = scores * inverse + spread[g * TILE : (g + 1) * TILE]
        tops = [
            jnp.max(jnp.where(even if h == 0 else ~even, scores, -jnp.inf), axis=1, keepdims=True)
            for h in range(2)
        ]
        weights = jnp.exp(scores - jnp.where(even, tops[0], tops[1])).astype(BF16).astype(F32)
        parts = [jnp.where(even, weights, 0.0), jnp.where(even, 0.0, weights)]
        sums = [row_sum(part) for part in parts]
        both_parts = jnp.concatenate(parts).astype(BF16)
        mixed = [jnp.zeros((TILE, LANES), F32) for _ in range(2)]
        for i in range(GROUP):
            found = dot(both_parts, values[g * GROUP + i])
            for h in range(2):
                mixed[h] = jnp.where(sub == i, found[h * TILE : (h + 1) * TILE], mixed[h])
        for h in range(2):
            sa[g, h] = (mixed[h] / sums[h]).astype(BF16)
            stats = stats + as_line(tops[h] + jnp.log(sums[h]), ROWS * h + g * TILE)
    rst[y] = stats
    along_y(lambda far: rst.at[y], lambda near: rst.at[near], st_sems)
    along_y(lambda far: sa.at[far], lambda near: ra.at[near], a_sems)
    with jax.named_scope("y_merge"):
        from_y(lambda near: rst.at[near], st_sems)
        from_y(lambda near: ra.at[near], a_sems)

    def merged(levels, parts):
        top = functools.reduce(jnp.maximum, levels)
        shares = [jnp.exp(level - top) for level in levels]
        whole = sum(shares[1:], shares[0])
        value = sum((a * b for a, b in zip(shares[1:], parts[1:])), shares[0] * parts[0])
        return value / whole, top + jnp.log(whole)

    spots = [y] + [at_y(k) for k in y_steps]
    stats = jnp.zeros((1, LANES), F32)
    for h in range(2):
        levels = [column(rst[spot], ROWS * h + y * TILE) for spot in spots]
        parts = [sa[y, h].astype(F32)] + [ra[spot, h].astype(F32) for spot in spots[1:]]
        value, level = merged(levels, parts)
        za[z, h] = value.astype(BF16)
        stats = stats + as_line(level, ROWS * h)
    zst[z] = stats
    along_z(zst, zst_sems)
    along_z(za, za_sems)

    with jax.named_scope("z_keyvalue"):
        from_z(zkv, zkv_sems)
    both = zkv[0].astype(F32)
    for k in range(1, depth):
        both = both + zkv[k].astype(F32)
    fresh = [jnp.where(sub < GROUP, factor * both[u], 0.0).astype(BF16).astype(F32) for u in range(4)]
    own_level = [row_sum(query[h].astype(F32) * fresh[h]) * inverse for h in range(2)]
    from_y(lambda near: first_all.at[near], first_sems)
    from_y(lambda near: gates_b_all.at[:, :, near], gates_b_sems)
    from_y(lambda near: down_b_all.at[:, near], down_b_sems)
    from_y(lambda near: wo_all.at[near], wo_sems)
    with jax.named_scope("z_merge"):
        from_z(zst, zst_sems)
        from_z(za, za_sems)
    attended = []
    for h in range(2):
        levels = [column(zst[k], ROWS * h) + log_gate[h] for k in range(depth)] + [own_level[h]]
        parts = [za[k, h].astype(F32) for k in range(depth)] + [fresh[2 + h]]
        attended.append(merged(levels, parts)[0])
    attended = jnp.concatenate(attended, axis=1).astype(BF16)
    send_two, got_two, two_sems = t_two
    mine = dot_rows(attended, wo_all[...].reshape(slab, 2 * LANES)).astype(BF16)
    send_two[...] = mine
    got_two[y, tp] = mine
    over_plane(lambda far: send_two, got_two, two_sems)
    with jax.named_scope("plane_two"):
        from_plane(got_two, two_sems)

    mixed = jnp.concatenate(
        [(first_all[g].astype(F32) + added(got_two.at[g])).astype(BF16).astype(F32) for g in range(SIDE)]
    )
    scaled = (mixed * gain_b_slab).astype(BF16)
    squares = jnp.broadcast_to(as_line(row_sum(mixed * mixed), 0), (TILE, LANES))
    sz = ff_b[0]
    for n in range(share):
        for u in range(2):
            product = dot(scaled, gates_b_all[n, u].reshape(slab, LANES))
            for g in range(SIDE):
                tile = product[g * TILE : (g + 1) * TILE]
                if u == 0:
                    tile = jnp.where(sub == GROUP, squares, tile)
                sz[n * SIDE + g, u] = tile.astype(BF16)
        send_pieces(ff_b, n)
    lower = jnp.where(iota((slab, width), 0) == iota((slab, width), 1) + y * width, 1.0, 0.0).astype(BF16)
    residual = dot(mixed.astype(BF16), lower)
    hidden = hidden_units(ff_b)
    send_three, got_three, three_sems = t_three
    for g in range(SIDE):
        partial = jnp.zeros((ROWS, width), F32)
        for n in range(share):
            partial = partial + dot_rows(hidden[n], down_b_all[n, g])
        send_three[g] = partial.astype(BF16)
    got_three[y, tp] = send_three[y]
    over_plane(lambda far: send_three.at[far], got_three, three_sems)
    with jax.named_scope("plane_three"):
        from_plane(got_three, three_sems)
    summed = sum((added(got_three.at[g]) for g in range(1, SIDE)), added(got_three.at[0]))
    last = (residual + 0.5 * summed).astype(BF16)

    back = iota((seqs, ROWS), 1)
    seat = lax.shift_right_logical(back, 3) * GROUP + (back & 7)
    lift = jnp.where(((back & 7) < GROUP) & (seat == iota((seqs, ROWS), 0)), 1.0, 0.0).astype(BF16)
    out_ref[...] = dot(lift, last).astype(BF16)

    for condition, copy in sent:
        if condition is None:
            copy.wait_send()
        else:
            ref, sem = copy

            @pl.when(condition)
            def _():
                await_slot(ref, sem)


def on_device(
    ranks,
    tokens,
    gain_first,
    gate_first,
    up_first,
    down_first,
    gain_mixer,
    query_weight,
    key_weight,
    value_weight,
    forget_weight,
    forget_bias,
    key_cache,
    value_cache,
    forget_sum,
    out_weight,
    gain_second,
    gate_second,
    up_second,
    down_second,
):
    kv_count, tp_count = ranks
    depth = kv_count // SIDE
    seqs, length = key_cache.shape[:2]
    chunks = gate_first.shape[1] // LANES
    share = -(-chunks // SIDE)
    pieces = share * SIDE
    width = tokens.shape[1]
    slab = SIDE * width
    dma = pltpu.SemaphoreType.DMA

    def flat(cache):
        return cache.reshape(seqs, 2 * length, LANES)

    operands = [
        tokens,
        gain_first.reshape(1, -1),
        gate_first,
        up_first,
        down_first.T,
        gain_mixer.reshape(1, -1),
        query_weight,
        key_weight,
        value_weight,
        forget_weight.T,
        flat(key_cache),
        flat(value_cache),
        forget_sum,
        out_weight.T,
        gain_second.reshape(1, -1),
        gate_second,
        up_second,
        down_second.T,
    ]

    def half(*dims):
        return pltpu.VMEM(dims, BF16)

    def tiles(*dims):
        return pltpu.VMEM((*dims, TILE, LANES), BF16)

    def pair(count, other=None):
        return (dma((count,)), dma((other or count,)))

    def ff():
        return (tiles(pieces, 2), tiles(depth, 2), tiles(pieces), pair(depth), pair(depth, pieces))

    def plane():
        return (dma((SIDE * tp_count,)), dma((SIDE, tp_count)))

    held = [
        half(seqs, width),
        half(1, width),
        half(*gate_first.shape),
        half(*up_first.shape),
        half(1, width),
        half(1, width),
        half(forget_weight.shape[1], slab),
        half(seqs, 2 * length, LANES),
        half(seqs, 2 * length, LANES),
        pltpu.VMEM(forget_sum.shape, F32),
        half(pieces, width, LANES),
        half(pieces, 2, width, LANES),
        half(pieces, width, LANES),
        half(3, SIDE, width, 2 * LANES),
        half(SIDE, width, 2 * LANES),
        half(share, SIDE, width, LANES),
        half(share, 2, SIDE, width, LANES),
        half(share, SIDE, width, LANES),
        dma((4 + 1 + 1 + chunks + 1 + 3 + 1 + 1 + 1 + 1 + 3 * chunks,)),
        half(SIDE, TILE, width),
        half(SIDE, TILE, width),
        tiles(SIDE, pieces, 2),
        tiles(SIDE, pieces, 2),
        ff(),
        ff(),
        (
            tiles(depth, 2),
            tiles(depth, 4),
            tiles(SIDE, 2),
            tiles(SIDE, 2),
            tiles(SIDE, 2),
            pltpu.VMEM((SIDE, 1, LANES), F32),
            tiles(depth, 2),
            pltpu.VMEM((depth, 1, LANES), F32),
            pair(depth),
            pair(depth),
            pair(SIDE),
            pair(SIDE),
            pair(SIDE),
            pair(depth),
            pair(depth),
        ),
        (half(SIDE, TILE, slab), half(SIDE, tp_count, TILE, slab), plane()),
        (half(TILE, slab), half(SIDE, tp_count, TILE, slab), plane()),
        (half(SIDE, ROWS, width), half(SIDE, tp_count, ROWS, width), plane()),
        half(SIDE, TILE, slab),
        pair(SIDE),
        (dma((share, SIDE)), dma((share, SIDE))),
        pair(SIDE),
        (dma((3, SIDE)), dma((3, SIDE))),
        pair(SIDE),
        pair(SIDE),
        pair(SIDE),
        pair(SIDE),
    ]
    return pl.pallas_call(
        functools.partial(layer_kernel, ranks, width * kv_count),
        out_shape=jax.ShapeDtypeStruct(tokens.shape, BF16),
        in_specs=[pl.BlockSpec(memory_space=pltpu.SMEM)]
        + [pl.BlockSpec(memory_space=pltpu.HBM)] * len(operands),
        out_specs=pl.BlockSpec(memory_space=pltpu.VMEM),
        scratch_shapes=held,
        compiler_params=pltpu.CompilerParams(
            collective_id=0, has_side_effects=True, vmem_limit_bytes=67_043_328
        ),
        name="layer",
    )(forget_bias, *operands)


def solution(mesh):
    ranks = (mesh.shape["kv"], mesh.shape["tp"])
    kv, tp = "kv", "tp"
    in_specs = (
        P(None, kv),
        P(kv),
        P(kv, tp),
        P(kv, tp),
        P(tp, kv),
        P(kv),
        P(kv, tp),
        P(kv, tp),
        P(kv, tp),
        P(),
        P(),
        P(None, kv, tp, None),
        P(None, kv, tp, None),
        P(None, tp, kv),
        P(tp, kv),
        P(kv),
        P(kv, tp),
        P(kv, tp),
        P(tp, kv),
    )
    return jax.shard_map(
        functools.partial(on_device, ranks),
        mesh=mesh,
        in_specs=in_specs,
        out_specs=P(None, kv),
        check_vma=False,
    )
```

time: 125 us -> 101 us (0.81)
  local copies, waits for them, and re-layouts: 16.9 us -> 1.29 us
  Pallas kernels: 108 us -> 99 us
    unnamed x39 -> x1, local copies, waits for them, and re-layouts: 16.9 us -> 1.29 us
    pallas_call x1, Pallas kernels: 108 us -> 99 us  [on_device(): pl.pallas_call(functools.partial(layer_kernel, ranks, width * kv_count),...]
where the time goes in v2:
time: 101 us; the launch traced here: 100 us
  Pallas kernels  99 us (98%)
  local copies, waits for them, and re-layouts  1.29 us (1%)
    pallas_call x1, Pallas kernels, on_device(): pl.pallas_call(functools.partial(layer_kernel, ranks, width * kv_count),...  99 us

profile of v2, /device:TPU:1, one launch (start us, length us, event | category | flops | bytes accessed | tf_op | source)
XLA Modules:
  0.0 100.3 jit_solution(12371295552247359896)
XLA Ops:
  0.0 99.0 %layer.1 = bf16[24,64]{1,0:T(8,128)(2,1)} custom-call(f32[16]{0:T(128)} %bias.1, bf16[24,64]{1,0:T(8,128)(2,1)} %tokens_hbm.1, bf16[1,64]{1,0:T(2,128)(2,1)} %bitcast.15, bf16[64,1408]{1,0:T(8,128)(2,1)} %gate_a_hbm.1, bf16[64,1408]{1,0:T(8,128)(2,1)} %up_a_hbm.1, bf16[64,1408]{1,0:T(8,128)(2,1)} %bitcast.11, bf16[1,64]{1,0:T(2,128)(2,1)} %bitcast.16, ...), custom_call_target="tpu_custom_call" | custom-call | tf_op jit(solution)/shard_map/layer/pallas_call | solution.py:712
  99.0 1.3 %copy.21 = bf16[24,64]{1,0:T(8,128)(2,1)} copy(bf16[24,64]{1,0:T(8,128)(2,1)} %layer.1) | data formatting | bytes 6144

commit v3 on v2

v3 whole, which is shorter than its diff:
```python
import functools

import jax
import jax.numpy as jnp
from jax import lax
from jax.experimental import pallas as pl
from jax.experimental.pallas import tpu as pltpu
from jax.sharding import PartitionSpec as P

MESH = pl.DeviceIdType.MESH
EPSILON = 1e-06
SIDE = 4
GROUP = 6
TILE = 8
ROWS = SIDE * TILE
LANES = 128
F32 = jnp.float32
BF16 = jnp.bfloat16


def dot(left, right):
    return lax.dot_general(left, right, (((1,), (0,)), ((), ())), preferred_element_type=F32)


def dot_rows(left, right):
    return lax.dot_general(left, right, (((1,), (1,)), ((), ())), preferred_element_type=F32)


def iota(shape, dim):
    return lax.broadcasted_iota(jnp.int32, shape, dim)


def far_first(count):
    return sorted(range(1, count), key=lambda k: (-min(k, count - k), k))


def split_value(value, pieces):
    parts = []
    for _ in range(pieces):
        part = value.astype(BF16)
        parts.append(part)
        value = value - part.astype(F32)
    return parts


def layer_kernel(
    ranks,
    features,
    bias_hbm,
    tokens_hbm,
    gain_a_hbm,
    gate_a_hbm,
    up_a_hbm,
    down_a_hbm,
    gain_m_hbm,
    wq_hbm,
    wk_hbm,
    wv_hbm,
    forget_hbm,
    keys_hbm,
    values_hbm,
    decay_hbm,
    wo_hbm,
    gain_b_hbm,
    gate_b_hbm,
    up_b_hbm,
    down_b_hbm,
    out_ref,
    bias,
    tokens,
    gain_a,
    gate_a,
    up_a,
    gain_m,
    gain_b,
    forget,
    keys,
    values,
    decay,
    down_a,
    gates_b,
    down_b,
    w_all,
    wo_all,
    down_a_all,
    gates_b_all,
    down_b_all,
    sems,
    tiles_y,
    tiles_all,
    sy,
    ry,
    ff_a,
    ff_b,
    mix_bufs,
    t_one,
    t_two,
    t_three,
    first_all,
    spread,
):
    kv_count, tp_count = ranks
    depth = kv_count // SIDE
    kv, tp = lax.axis_index("kv"), lax.axis_index("tp")
    z, y = lax.div(kv, SIDE), lax.rem(kv, SIDE)
    chunks = gate_a.shape[1] // LANES
    share = down_a.shape[0] // SIDE
    pieces = share * SIDE
    width = tokens.shape[1]
    slab = SIDE * width
    seqs = tokens.shape[0]
    positions = decay.shape[2]

    def at_z(k):
        return lax.rem(z + k, depth)

    def at_y(k):
        return lax.rem(y + k, SIDE)

    def at_tp(k):
        return lax.rem(tp + k, tp_count)

    z_steps, y_steps = far_first(depth), far_first(SIDE)
    plane = sorted(
        [(a, b) for a in range(SIDE) for b in range(tp_count) if a or b],
        key=lambda s: (-min(s[0], SIDE - s[0]) - min(s[1], tp_count - s[1]) / 2, s),
    )

    counter = iter(range(sems.shape[0]))

    def fresh_sem():
        return sems.at[next(counter)]

    def fresh_pair():
        return fresh_sem(), fresh_sem()

    def take(ref, sem):
        pltpu.make_async_copy(ref, ref, sem).wait()

    barrier = pltpu.get_barrier_semaphore()
    for k in z_steps:
        pl.semaphore_signal(barrier, inc=1, device_id=(at_z(k) * SIDE + y, tp), device_id_type=MESH)

    def columns(ref, j):
        return ref.at[:, pl.ds(j * LANES, LANES)]

    loads = {}

    def load(name, whole, *copies):
        sem = fresh_sem()
        for source, target in copies:
            pltpu.make_async_copy(source, target, sem).start()
        loads[name] = (whole, sem)

    def load_one(name, source, target):
        load(name, target, (source, target))

    def loaded(*names):
        for name in names:
            take(*loads.pop(name))

    load_one("tokens", tokens_hbm, tokens)
    load_one("gain_a", gain_a_hbm, gain_a)
    load_one("gate_a", gate_a_hbm, gate_a)
    load_one("up_a", up_a_hbm, up_a)
    load_one("gain_m", gain_m_hbm, gain_m)
    load_one("gain_b", gain_b_hbm, gain_b)
    for a, b in plane:
        pl.semaphore_signal(barrier, inc=1, device_id=(z * SIDE + at_y(a), at_tp(b)), device_id_type=MESH)
    load("down_a", down_a.at[pl.ds(0, chunks)], *[(columns(down_a_hbm, j), down_a.at[j]) for j in range(chunks)])
    load(
        "w",
        w_all.at[:, y],
        (wq_hbm, w_all.at[0, y]),
        (wk_hbm, w_all.at[1, y]),
        (wv_hbm, w_all.at[2, y]),
    )
    load_one("wo", wo_hbm, wo_all.at[y])
    load_one("decay", decay_hbm, decay)
    load_one("bias", bias_hbm, bias)
    load_one("forget", forget_hbm.at[:, pl.ds(pl.multiple_of(z * slab, slab), slab)], forget)
    load_one("keys", keys_hbm, keys)
    load_one("values", values_hbm, values)
    load(
        "gates_b",
        gates_b.at[pl.ds(0, chunks)],
        *[(columns(gate_b_hbm, j), gates_b.at[j, 0]) for j in range(chunks)],
        *[(columns(up_b_hbm, j), gates_b.at[j, 1]) for j in range(chunks)],
    )
    load("down_b", down_b.at[pl.ds(0, chunks)], *[(columns(down_b_hbm, j), down_b.at[j]) for j in range(chunks)])

    sent = []

    def push(source, target, sems, device):
        pltpu.make_async_remote_copy(
            src_ref=source,
            dst_ref=target,
            send_sem=sems[0],
            recv_sem=sems[1],
            device_id=device,
            device_id_type=MESH,
        ).start()

    def along_y(source_of, target_of, three):
        sems = fresh_pair()
        for k in y_steps:
            far = at_y(k)
            push(source_of(far), target_of(y), sems, (z * SIDE + far, tp))
        sent.append((None, three, sems[0]))
        return lambda: take(three, sems[1])

    def along_z(target):
        sems = fresh_pair()
        for k in z_steps:
            push(target.at[z], target.at[z], sems, (at_z(k) * SIDE + y, tp))
        others = target.at[pl.ds(0, depth - 1)]
        sent.append((None, others, sems[0]))
        return lambda: take(others, sems[1])

    def over_plane(source_of, target):
        sems = fresh_pair()
        for a, b in plane:
            far = at_y(a)
            push(source_of(far), target.at[y * tp_count + tp], sems, (z * SIDE + far, at_tp(b)))
        others = target.at[pl.ds(0, SIDE * tp_count - 1)]
        sent.append((None, others, sems[0]))
        return lambda: take(others, sems[1])

    sub, lane = iota((TILE, LANES), 0), iota((TILE, LANES), 1)

    def column(line, first):
        picked = jnp.where(lane == first + sub, jnp.broadcast_to(line, (TILE, LANES)), 0.0)
        return jnp.sum(picked, axis=1, keepdims=True)

    def as_line(values, first):
        shape = (values.shape[0], LANES)
        spread_out = jnp.where(iota(shape, 1) == first + iota(shape, 0), values, 0.0)
        return jnp.sum(spread_out, axis=0, keepdims=True)

    def row_sum(x):
        return jnp.sum(x, axis=1, keepdims=True)

    def owner(p):
        return lax.div(p * depth, pieces)

    def piece_of(place):
        return lax.div(pieces * place + depth - 1, depth)

    def owns(place):
        p = piece_of(place)
        return jnp.logical_and(p < pieces, owner(p) == place)

    def send_pieces(bufs, sems, n):
        sz, rz, hz = bufs
        for k in z_steps:
            far = at_z(k)
            p = piece_of(far)

            @pl.when(jnp.logical_and(owns(far), lax.div(p, SIDE) == n))
            def _():
                push(sz.at[p], rz.at[z], sems, (far * SIDE + y, tp))

    def hidden_units(bufs, rs_sems):
        sz, rz, hz = bufs
        ag_sems = fresh_pair()
        mine_too = jnp.logical_not(owns(z))
        sent.append((owns(z), sz.at[pl.ds(0, pieces - 1)], rs_sems[0]))
        sent.append((mine_too, sz, rs_sems[0]))

        @pl.when(owns(z))
        def _():
            mine = piece_of(z)
            with jax.named_scope("z_reduce"):
                take(rz.at[pl.ds(0, depth - 1)], rs_sems[1])
            rz[z] = sz[mine]
            both = rz[0].astype(F32)
            for k in range(1, depth):
                both = both + rz[k].astype(F32)
            gate_sum, up_sum = both[0], both[1]
            factor = lax.rsqrt(gate_sum[GROUP : GROUP + 1] / features + EPSILON)
            factor = column(factor, lax.rem(mine, SIDE) * TILE)
            gate_value, up_value = factor * gate_sum, factor * up_sum
            hidden = gate_value / (1.0 + jnp.exp(-gate_value)) * up_value
            hz[mine] = jnp.where(sub < GROUP, hidden, 0.0).astype(BF16)
            for k in z_steps:
                push(hz.at[mine], hz.at[mine], ag_sems, (at_z(k) * SIDE + y, tp))

        sent.append((owns(z), rz.at[pl.ds(0, depth - 1), 0], ag_sems[0]))
        with jax.named_scope("z_gather"):

            @pl.when(owns(z))
            def _():
                take(hz.at[pl.ds(0, pieces - 1)], ag_sems[1])

            @pl.when(mine_too)
            def _():
                take(hz, ag_sems[1])

        return [
            hz[n * SIDE : (n + 1) * SIDE].astype(F32).reshape(ROWS, LANES).astype(BF16) for n in range(share)
        ]

    to_rows = iota((ROWS, seqs), 0)
    seat = lax.shift_right_logical(to_rows, 3) * GROUP + (to_rows & 7)
    place = jnp.where(((to_rows & 7) < GROUP) & (seat == iota((ROWS, seqs), 1)), 1.0, 0.0).astype(BF16)

    loaded("tokens", "gain_a", "gain_m", "gain_b")
    x = dot(place, tokens[...])
    gain_rows = [jnp.broadcast_to(g[...].astype(F32), (ROWS, width)) for g in (gain_m, gain_b)]
    row_in_tile = iota((ROWS, width), 0) & 7
    with_gains = jnp.where(row_in_tile == GROUP, gain_rows[0], jnp.where(row_in_tile == GROUP + 1, gain_rows[1], x))
    for g in range(SIDE):
        tiles_y[g] = with_gains[g * TILE : (g + 1) * TILE].astype(BF16)
    tiles_all[y] = tiles_y[y]

    scaled = (x * gain_a[...].astype(F32)).astype(BF16)
    squares = jnp.broadcast_to(as_line(row_sum(x * x), 0), (TILE, LANES))
    loaded("gate_a", "up_a")
    for u, weight in enumerate((gate_a, up_a)):
        product = dot(scaled, weight[...])
        for j in range(chunks):
            for g in range(SIDE):
                tile = product[g * TILE : (g + 1) * TILE, j * LANES : (j + 1) * LANES]
                if u == 0:
                    tile = jnp.where(sub == GROUP, squares, tile)
                sy[j // share, (j % share) * SIDE + g, u] = tile.astype(BF16)
    for j in range(chunks, pieces):
        for g in range(SIDE):
            for u in range(2):
                sy[j // share, (j % share) * SIDE + g, u] = jnp.zeros((TILE, LANES), BF16)
        down_a[j] = jnp.zeros((width, LANES), BF16)
        for u in range(2):
            gates_b[j, u] = jnp.zeros((width, LANES), BF16)
        down_b[j] = jnp.zeros((width, LANES), BF16)

    with jax.named_scope("barrier"):
        pl.semaphore_wait(barrier, len(z_steps) + len(plane))

    def portion(ref, which, n):
        return ref.at[which, pl.ds(n * SIDE, SIDE)]

    first_three = pl.ds(0, SIDE - 1)
    reduced = [
        along_y(lambda far: portion(sy, far, n), lambda near: portion(ry, near, n), portion(ry, first_three, n))
        for n in range(share)
    ]
    tiles_here = along_y(lambda far: tiles_y.at[far], lambda near: tiles_all.at[near], tiles_all.at[first_three])
    loaded("down_a")
    down_a_here = along_y(
        lambda far: down_a.at[pl.ds(far * share, share)],
        lambda near: down_a_all.at[:, near],
        down_a_all.at[:, first_three],
    )
    down_a_all[:, y] = down_a[pl.ds(y * share, share)]
    loaded("w")
    w_here = along_y(lambda far: w_all.at[:, y], lambda near: w_all.at[:, near], w_all.at[:, first_three])
    loaded("wo")
    wo_here = along_y(lambda far: wo_all.at[y], lambda near: wo_all.at[near], wo_all.at[first_three])

    loaded("down_b")
    down_b_here = along_y(
        lambda far: down_b.at[pl.ds(far * share, share)],
        lambda near: down_b_all.at[:, near],
        down_b_all.at[:, first_three],
    )

    sz, ff_sems = ff_a[0], fresh_pair()
    for n in range(share):
        with jax.named_scope("y_reduce"):
            reduced[n]()
        rows = pl.ds(n * SIDE, SIDE)
        total = sy[y, rows].astype(F32)
        for k in y_steps:
            total = total + ry[at_y(k), rows].astype(F32)
        sz[rows] = total.astype(BF16)
        send_pieces(ff_a, ff_sems, n)

    loaded("decay")
    woven_all = jnp.zeros((ROWS, 2 * positions), F32)
    thirds = [split_value(decay[:, h, :], 3) for h in range(2)]
    for n in range(3):
        woven = jnp.zeros((seqs, 2 * positions), F32)
        for h in range(2):
            weave = jnp.where(
                iota((positions, 2 * positions), 1) == 2 * iota((positions, 2 * positions), 0) + h, 1.0, 0.0
            ).astype(BF16)
            woven = woven + dot(thirds[h][n], weave)
        woven_all = woven_all + dot(place, woven.astype(BF16))
    for g in range(SIDE):
        spread[g] = woven_all[g * TILE : (g + 1) * TILE]
    tiles_here()
    own_rows = jnp.zeros((TILE, slab), F32)
    for g in range(SIDE):
        lift = jnp.where(iota((width, slab), 1) == iota((width, slab), 0) + g * width, 1.0, 0.0).astype(BF16)
        own_rows = own_rows + dot(tiles_all[g], lift)
    gain_m_slab, gain_b_slab = own_rows[GROUP : GROUP + 1], own_rows[GROUP + 1 : GROUP + 2]
    wide = iota((TILE, slab), 0) < GROUP
    own_rows = jnp.where(wide, own_rows, 0.0)

    hidden = hidden_units(ff_a, ff_sems)
    down_a_here()
    partial = jnp.zeros((ROWS, slab), F32)
    for n in range(share):
        partial = partial + dot_rows(hidden[n], down_a_all[n].reshape(slab, LANES))
    send_one, got_one = t_one
    for g in range(SIDE):
        send_one[g] = partial[g * TILE : (g + 1) * TILE].astype(BF16)
    got_one[y * tp_count + tp] = send_one[y]
    one_here = over_plane(lambda far: send_one.at[far], got_one)
    loaded("gates_b")
    with jax.named_scope("plane_one"):
        one_here()

    def added(ref, first, count):
        total = ref[first].astype(F32)
        for k in range(1, count):
            total = total + ref[first + k].astype(F32)
        return total

    summed = added(got_one, 0, SIDE * tp_count)
    first_rows = (own_rows + 0.5 * summed).astype(BF16)
    first_all[y] = first_rows

    zq, zkv, qf, sa, ra, own_stats, rst, za, zst = mix_bufs
    inverse = LANES ** (-0.5)
    x = first_rows.astype(F32)
    scaled = (x * gain_m_slab).astype(BF16)
    loaded("forget", "bias")
    heads = forget.shape[0]
    r8, c8 = iota((TILE, heads), 0), iota((TILE, heads), 1)
    pick = jnp.where((r8 < 2) & (c8 == 2 * tp + r8), 1.0, 0.0).astype(BF16)
    lines = dot(pick, forget[...])
    biases = row_sum(jnp.where((r8 < 2) & (c8 == 2 * tp + r8), jnp.broadcast_to(bias[...], (TILE, heads)), 0.0))
    side_line = as_line(row_sum(x * x), 0)
    for h in range(2):
        side_line = side_line + as_line(row_sum(scaled.astype(F32) * lines[h : h + 1]), ROWS * (h + 1))
    side_line = jnp.broadcast_to(side_line, (TILE, LANES))
    with jax.named_scope("w_wait"):
        w_here()
    product = [dot(scaled, w_all[u].reshape(slab, 2 * LANES)) for u in range(3)]
    for h in range(2):
        tile = product[0][:, h * LANES : (h + 1) * LANES]
        zq[z, h] = (jnp.where(sub == GROUP, side_line, tile) if h == 0 else tile).astype(BF16)
    zq_here = along_z(zq)
    for u in range(2):
        for h in range(2):
            zkv[z, 2 * u + h] = product[1 + u][:, h * LANES : (h + 1) * LANES].astype(BF16)
    first_here = along_y(lambda far: first_all.at[y], lambda near: first_all.at[near], first_all.at[first_three])
    gates_b_here = along_y(
        lambda far: gates_b.at[pl.ds(far * share, share)],
        lambda near: gates_b_all.at[:, :, near],
        gates_b_all.at[:, :, first_three],
    )
    gates_b_all[:, :, y] = gates_b[pl.ds(y * share, share)]
    down_b_all[:, y] = down_b[pl.ds(y * share, share)]

    with jax.named_scope("z_query"):
        zq_here()
    both = zq[0].astype(F32)
    for k in range(1, depth):
        both = both + zq[k].astype(F32)
    line = both[0][GROUP : GROUP + 1]
    factor = column(lax.rsqrt(line / features + EPSILON), 0)
    query = [jnp.where(sub < GROUP, factor * both[h], 0.0).astype(BF16) for h in range(2)]
    for h in range(2):
        qf[y, h] = query[h]
    qf_here = along_y(lambda far: qf.at[y], lambda near: qf.at[near], qf.at[first_three])
    zkv_here = along_z(zkv)
    log_gate = []
    for h in range(2):
        gate = factor * column(line, ROWS * (h + 1)) + biases[h : h + 1]
        log_gate.append(jnp.minimum(gate, 0.0) - jnp.log(1.0 + jnp.exp(-jnp.abs(gate))))
    loaded("keys", "values")

    with jax.named_scope("y_query"):
        qf_here()
    lane2, sub2 = iota((TILE, 2 * positions), 1), iota((TILE, 2 * positions), 0)
    even = lax.rem(lane2, 2) == 0
    ra_sems, rst_sems = fresh_pair(), fresh_pair()
    for k in [*y_steps, 0]:
        g = at_y(k)
        stats = jnp.zeros((1, LANES), F32)
        pair = jnp.concatenate([qf[g, 0].astype(F32), qf[g, 1].astype(F32)]).astype(BF16)
        scores = jnp.zeros((TILE, 2 * positions), F32)
        for i in range(GROUP):
            found = dot_rows(pair, keys[g * GROUP + i])
            found = jnp.where(even, found[:TILE], found[TILE:])
            scores = jnp.where(sub2 == i, found, scores)
        scores = scores * inverse + spread[g]
        tops = [
            jnp.max(jnp.where(even if h == 0 else ~even, scores, -jnp.inf), axis=1, keepdims=True)
            for h in range(2)
        ]
        weights = jnp.exp(scores - jnp.where(even, tops[0], tops[1])).astype(BF16).astype(F32)
        parts = [jnp.where(even, weights, 0.0), jnp.where(even, 0.0, weights)]
        sums = [row_sum(part) for part in parts]
        both_parts = jnp.concatenate(parts).astype(BF16)
        mixed = [jnp.zeros((TILE, LANES), F32) for _ in range(2)]
        for i in range(GROUP):
            found = dot(both_parts, values[g * GROUP + i])
            for h in range(2):
                mixed[h] = jnp.where(sub == i, found[h * TILE : (h + 1) * TILE], mixed[h])
        for h in range(2):
            sa[g, h] = (mixed[h] / sums[h]).astype(BF16)
            stats = stats + as_line(tops[h] + jnp.log(sums[h]), ROWS * h)
        own_stats[g] = stats
        if k:
            push(own_stats.at[g], rst.at[y], rst_sems, (z * SIDE + g, tp))
            push(sa.at[g], ra.at[y], ra_sems, (z * SIDE + g, tp))
    sent.append((None, ra.at[first_three], ra_sems[0]))
    sent.append((None, rst.at[first_three], rst_sems[0]))
    with jax.named_scope("y_merge"):
        take(rst.at[first_three], rst_sems[1])
        take(ra.at[first_three], ra_sems[1])

    def merged(levels, parts):
        top = functools.reduce(jnp.maximum, levels)
        shares = [jnp.exp(level - top) for level in levels]
        whole = sum(shares[1:], shares[0])
        value = sum((a * b for a, b in zip(shares[1:], parts[1:])), shares[0] * parts[0])
        return value / whole, top + jnp.log(whole)

    spots = [y] + [at_y(k) for k in y_steps]
    stats = jnp.zeros((1, LANES), F32)
    for h in range(2):
        levels = [column(own_stats[y], ROWS * h)] + [column(rst[spot], ROWS * h) for spot in spots[1:]]
        parts = [sa[y, h].astype(F32)] + [ra[spot, h].astype(F32) for spot in spots[1:]]
        value, level = merged(levels, parts)
        za[z, h] = value.astype(BF16)
        stats = stats + as_line(level, ROWS * h)
    zst[z] = stats
    zst_here = along_z(zst)
    za_here = along_z(za)

    with jax.named_scope("z_keyvalue"):
        zkv_here()
    both = zkv[0].astype(F32)
    for k in range(1, depth):
        both = both + zkv[k].astype(F32)
    fresh = [jnp.where(sub < GROUP, factor * both[u], 0.0).astype(BF16).astype(F32) for u in range(4)]
    own_level = [row_sum(query[h].astype(F32) * fresh[h]) * inverse for h in range(2)]
    first_here()
    gates_b_here()
    down_b_here()
    wo_here()
    with jax.named_scope("z_merge"):
        zst_here()
        za_here()
    attended = []
    for h in range(2):
        levels = [column(zst[k], ROWS * h) + log_gate[h] for k in range(depth)] + [own_level[h]]
        parts = [za[k, h].astype(F32) for k in range(depth)] + [fresh[2 + h]]
        attended.append(merged(levels, parts)[0])
    attended = jnp.concatenate(attended, axis=1).astype(BF16)
    send_two, got_two = t_two
    mine = dot_rows(attended, wo_all[...].reshape(slab, 2 * LANES)).astype(BF16)
    send_two[...] = mine
    got_two[y * tp_count + tp] = mine
    two_here = over_plane(lambda far: send_two, got_two)
    with jax.named_scope("plane_two"):
        two_here()

    mixed = jnp.concatenate(
        [(first_all[g].astype(F32) + added(got_two, g * tp_count, tp_count)).astype(BF16).astype(F32) for g in range(SIDE)]
    )
    scaled = (mixed * gain_b_slab).astype(BF16)
    squares = jnp.broadcast_to(as_line(row_sum(mixed * mixed), 0), (TILE, LANES))
    sz, ff_sems = ff_b[0], fresh_pair()
    for n in range(share):
        for u in range(2):
            product = dot(scaled, gates_b_all[n, u].reshape(slab, LANES))
            for g in range(SIDE):
                tile = product[g * TILE : (g + 1) * TILE]
                if u == 0:
                    tile = jnp.where(sub == GROUP, squares, tile)
                sz[n * SIDE + g, u] = tile.astype(BF16)
        send_pieces(ff_b, ff_sems, n)
    lower = jnp.where(iota((slab, width), 0) == iota((slab, width), 1) + y * width, 1.0, 0.0).astype(BF16)
    residual = dot(mixed.astype(BF16), lower)
    hidden = hidden_units(ff_b, ff_sems)
    send_three, got_three = t_three
    for g in range(SIDE):
        partial = jnp.zeros((ROWS, width), F32)
        for n in range(share):
            partial = partial + dot_rows(hidden[n], down_b_all[n, g])
        send_three[g] = partial.astype(BF16)
    got_three[y * tp_count + tp] = send_three[y]
    three_here = over_plane(lambda far: send_three.at[far], got_three)
    with jax.named_scope("plane_three"):
        three_here()
    summed = added(got_three, 0, SIDE * tp_count)
    last = (residual + 0.5 * summed).astype(BF16)

    back = iota((seqs, ROWS), 1)
    seat = lax.shift_right_logical(back, 3) * GROUP + (back & 7)
    lift = jnp.where(((back & 7) < GROUP) & (seat == iota((seqs, ROWS), 0)), 1.0, 0.0).astype(BF16)
    out_ref[...] = dot(lift, last).astype(BF16)

    for condition, ref, sem in sent:
        if condition is None:
            take(ref, sem)
        else:

            @pl.when(condition)
            def _():
                take(ref, sem)


def on_device(
    ranks,
    tokens,
    gain_first,
    gate_first,
    up_first,
    down_first,
    gain_mixer,
    query_weight,
    key_weight,
    value_weight,
    forget_weight,
    forget_bias,
    key_cache,
    value_cache,
    forget_sum,
    out_weight,
    gain_second,
    gate_second,
    up_second,
    down_second,
):
    kv_count, tp_count = ranks
    depth = kv_count // SIDE
    seqs, length = key_cache.shape[:2]
    chunks = gate_first.shape[1] // LANES
    share = -(-chunks // SIDE)
    pieces = share * SIDE
    width = tokens.shape[1]
    slab = SIDE * width
    dma = pltpu.SemaphoreType.DMA

    def flat(cache):
        return cache.reshape(seqs, 2 * length, LANES)

    operands = [
        tokens,
        gain_first.reshape(1, -1),
        gate_first,
        up_first,
        down_first.T,
        gain_mixer.reshape(1, -1),
        query_weight,
        key_weight,
        value_weight,
        forget_weight.T,
        flat(key_cache),
        flat(value_cache),
        forget_sum,
        out_weight.T,
        gain_second.reshape(1, -1),
        gate_second,
        up_second,
        down_second.T,
    ]

    def half(*dims):
        return pltpu.VMEM(dims, BF16)

    def tiles(*dims):
        return pltpu.VMEM((*dims, TILE, LANES), BF16)

    def ff():
        return (tiles(pieces, 2), tiles(depth, 2), tiles(pieces))

    held = [
        pltpu.VMEM((1, forget_weight.shape[1]), F32),
        half(seqs, width),
        half(1, width),
        half(*gate_first.shape),
        half(*up_first.shape),
        half(1, width),
        half(1, width),
        half(forget_weight.shape[1], slab),
        half(seqs, 2 * length, LANES),
        half(seqs, 2 * length, LANES),
        pltpu.VMEM(forget_sum.shape, F32),
        half(pieces, width, LANES),
        half(pieces, 2, width, LANES),
        half(pieces, width, LANES),
        half(3, SIDE, width, 2 * LANES),
        half(SIDE, width, 2 * LANES),
        half(share, SIDE, width, LANES),
        half(share, 2, SIDE, width, LANES),
        half(share, SIDE, width, LANES),
        dma((16 + 2 * (share + 21),)),
        half(SIDE, TILE, width),
        half(SIDE, TILE, width),
        tiles(SIDE, pieces, 2),
        tiles(SIDE, pieces, 2),
        ff(),
        ff(),
        (
            tiles(depth, 2),
            tiles(depth, 4),
            tiles(SIDE, 2),
            tiles(SIDE, 2),
            tiles(SIDE, 2),
            pltpu.VMEM((SIDE, 1, LANES), F32),
            pltpu.VMEM((SIDE, 1, LANES), F32),
            tiles(depth, 2),
            pltpu.VMEM((depth, 1, LANES), F32),
        ),
        (half(SIDE, TILE, slab), half(SIDE * tp_count, TILE, slab)),
        (half(TILE, slab), half(SIDE * tp_count, TILE, slab)),
        (half(SIDE, ROWS, width), half(SIDE * tp_count, ROWS, width)),
        half(SIDE, TILE, slab),
        pltpu.VMEM((SIDE, TILE, 2 * length), F32),
    ]
    return pl.pallas_call(
        functools.partial(layer_kernel, ranks, width * kv_count),
        out_shape=jax.ShapeDtypeStruct(tokens.shape, BF16),
        in_specs=[pl.BlockSpec(memory_space=pltpu.HBM)] * (1 + len(operands)),
        out_specs=pl.BlockSpec(memory_space=pltpu.VMEM),
        scratch_shapes=held,
        compiler_params=pltpu.CompilerParams(
            collective_id=0, has_side_effects=True, vmem_limit_bytes=67_043_328
        ),
        name="layer",
    )(forget_bias.reshape(1, -1), *operands)


def solution(mesh):
    ranks = (mesh.shape["kv"], mesh.shape["tp"])
    kv, tp = "kv", "tp"
    in_specs = (
        P(None, kv),
        P(kv),
        P(kv, tp),
        P(kv, tp),
        P(tp, kv),
        P(kv),
        P(kv, tp),
        P(kv, tp),
        P(kv, tp),
        P(),
        P(),
        P(None, kv, tp, None),
        P(None, kv, tp, None),
        P(None, tp, kv),
        P(tp, kv),
        P(kv),
        P(kv, tp),
        P(kv, tp),
        P(tp, kv),
    )
    return jax.shard_map(
        functools.partial(on_device, ranks),
        mesh=mesh,
        in_specs=in_specs,
        out_specs=P(None, kv),
        check_vma=False,
    )
```

time: 101 us -> 92.8 us (0.919)
  Pallas kernels: 99 us -> 91.3 us
    pallas_call x1, Pallas kernels: 99 us -> 91.3 us  [on_device(): pl.pallas_call(functools.partial(layer_kernel, ranks, width * kv_count),...]
where the time goes in v3:
time: 92.8 us; the launch traced here: 92.6 us
  Pallas kernels  91.3 us (98%)
  local copies, waits for them, and re-layouts  1.29 us (1%)
    pallas_call x1, Pallas kernels, on_device(): pl.pallas_call(functools.partial(layer_kernel, ranks, width * kv_count),...  91.3 us

profile of v3, /device:TPU:1, one launch (start us, length us, event | category | flops | bytes accessed | tf_op | source)
XLA Modules:
  0.0 92.6 jit_solution(16789275119177133479)
XLA Ops:
  0.0 91.3 %layer.1 = bf16[24,64]{1,0:T(8,128)(2,1)} custom-call(f32[1,16]{1,0:T(1,128)} %bitcast.16, bf16[24,64]{1,0:T(8,128)(2,1)} %tokens_hbm.1, bf16[1,64]{1,0:T(2,128)(2,1)} %bitcast.17, bf16[64,1408]{1,0:T(8,128)(2,1)} %gate_a_hbm.1, bf16[64,1408]{1,0:T(8,128)(2,1)} %up_a_hbm.1, bf16[64,1408]{1,0:T(8,128)(2,1)} %bitcast.12, bf16[1,64]{1,0:T(2,128)(2,1)} %bitcast.18, ...), custom_call_target="tpu_custom_call" | custom-call | tf_op jit(solution)/shard_map/layer/pallas_call | solution.py:718
  91.3 1.3 %copy.21 = bf16[24,64]{1,0:T(8,128)(2,1)} copy(bf16[24,64]{1,0:T(8,128)(2,1)} %layer.1) | data formatting | bytes 6144

commit v4 on v3

--- a/solution.py
+++ b/solution.py
@@ -86,6 +86,8 @@
     gates_b_all,
     down_b_all,
     sems,
+    entry_sems,
+    out_tile,
     tiles_y,
     tiles_all,
     sy,
@@ -138,8 +140,18 @@
         pltpu.make_async_copy(ref, ref, sem).wait()
 
     barrier = pltpu.get_barrier_semaphore()
+    near_sem, far_sem = entry_sems
+
+    def signal(sem, device):
+        pl.semaphore_signal(sem, inc=1, device_id=device, device_id_type=MESH)
+
     for k in z_steps:
-        pl.semaphore_signal(barrier, inc=1, device_id=(at_z(k) * SIDE + y, tp), device_id_type=MESH)
+        signal(barrier, (at_z(k) * SIDE, tp))
+    for k in y_steps:
+
+        @pl.when(at_y(k) != 0)
+        def _():
+            signal(barrier, (z * SIDE + at_y(k), tp))
 
     def columns(ref, j):
         return ref.at[:, pl.ds(j * LANES, LANES)]
@@ -165,8 +177,8 @@
     load_one("up_a", up_a_hbm, up_a)
     load_one("gain_m", gain_m_hbm, gain_m)
     load_one("gain_b", gain_b_hbm, gain_b)
-    for a, b in plane:
-        pl.semaphore_signal(barrier, inc=1, device_id=(z * SIDE + at_y(a), at_tp(b)), device_id_type=MESH)
+    for k in far_first(tp_count):
+        signal(barrier, (z * SIDE, at_tp(k)))
     load("down_a", down_a.at[pl.ds(0, chunks)], *[(columns(down_a_hbm, j), down_a.at[j]) for j in range(chunks)])
     load(
         "w",
@@ -201,6 +213,11 @@
             device_id_type=MESH,
         ).start()
 
+    filled = pl.ds(0, GROUP)
+
+    def rows_of(ref, which):
+        return ref.at[which, :, filled]
+
     def along_y(source_of, target_of, three):
         sems = fresh_pair()
         for k in y_steps:
@@ -209,20 +226,20 @@
         sent.append((None, three, sems[0]))
         return lambda: take(three, sems[1])
 
-    def along_z(target):
+    def along_z(target, view=lambda ref, which: ref.at[which]):
         sems = fresh_pair()
         for k in z_steps:
-            push(target.at[z], target.at[z], sems, (at_z(k) * SIDE + y, tp))
-        others = target.at[pl.ds(0, depth - 1)]
+            push(view(target, z), view(target, z), sems, (at_z(k) * SIDE + y, tp))
+        others = view(target, pl.ds(0, depth - 1))
         sent.append((None, others, sems[0]))
         return lambda: take(others, sems[1])
 
-    def over_plane(source_of, target):
+    def over_plane(source_of, target, view):
         sems = fresh_pair()
         for a, b in plane:
             far = at_y(a)
-            push(source_of(far), target.at[y * tp_count + tp], sems, (z * SIDE + far, at_tp(b)))
-        others = target.at[pl.ds(0, SIDE * tp_count - 1)]
+            push(source_of(far), view(target, y * tp_count + tp), sems, (z * SIDE + far, at_tp(b)))
+        others = view(target, pl.ds(0, SIDE * tp_count - 1))
         sent.append((None, others, sems[0]))
         return lambda: take(others, sems[1])
 
@@ -283,18 +300,18 @@
             hidden = gate_value / (1.0 + jnp.exp(-gate_value)) * up_value
             hz[mine] = jnp.where(sub < GROUP, hidden, 0.0).astype(BF16)
             for k in z_steps:
-                push(hz.at[mine], hz.at[mine], ag_sems, (at_z(k) * SIDE + y, tp))
-
-        sent.append((owns(z), rz.at[pl.ds(0, depth - 1), 0], ag_sems[0]))
+                push(hz.at[mine, filled], hz.at[mine, filled], ag_sems, (at_z(k) * SIDE + y, tp))
+
+        sent.append((owns(z), rz.at[pl.ds(0, depth - 1), 0, filled], ag_sems[0]))
         with jax.named_scope("z_gather"):
 
             @pl.when(owns(z))
             def _():
-                take(hz.at[pl.ds(0, pieces - 1)], ag_sems[1])
+                take(hz.at[pl.ds(0, pieces - 1), filled], ag_sems[1])
 
             @pl.when(mine_too)
             def _():
-                take(hz, ag_sems[1])
+                take(hz.at[:, filled], ag_sems[1])
 
         return [
             hz[n * SIDE : (n + 1) * SIDE].astype(F32).reshape(ROWS, LANES).astype(BF16) for n in range(share)
@@ -334,10 +351,19 @@
         down_b[j] = jnp.zeros((width, LANES), BF16)
 
     with jax.named_scope("barrier"):
-        pl.semaphore_wait(barrier, len(z_steps) + len(plane))
+
+        @pl.when(y != 0)
+        def _():
+            pl.semaphore_wait(barrier, len(y_steps))
+            signal(near_sem, (z * SIDE, tp))
+
+        @pl.when(y == 0)
+        def _():
+            pl.semaphore_wait(near_sem, len(y_steps))
+
 
     def portion(ref, which, n):
-        return ref.at[which, pl.ds(n * SIDE, SIDE)]
+        return ref.at[which, pl.ds(n * SIDE, SIDE), :, pl.ds(0, GROUP if n else TILE)]
 
     first_three = pl.ds(0, SIDE - 1)
     reduced = [
@@ -372,7 +398,24 @@
         total = sy[y, rows].astype(F32)
         for k in y_steps:
             total = total + ry[at_y(k), rows].astype(F32)
-        sz[rows] = total.astype(BF16)
+        if n == 0:
+            line = total[0, 0, GROUP : GROUP + 1]
+        gates = jnp.where(sub == GROUP, jnp.broadcast_to(line, (TILE, LANES)), total[:, 0])
+        sz[rows, 0] = gates.astype(BF16)
+        sz[rows, 1] = total[:, 1].astype(BF16)
+        if n == 0:
+            with jax.named_scope("barrier_far"):
+
+                @pl.when(y == 0)
+                def _():
+                    pl.semaphore_wait(barrier, SIDE * (len(z_steps) + tp_count - 1))
+                    for k in y_steps:
+                        signal(far_sem, (z * SIDE + at_y(k), tp))
+
+                @pl.when(y != 0)
+                def _():
+                    pl.semaphore_wait(far_sem, 1)
+
         send_pieces(ff_a, ff_sems, n)
 
     loaded("decay")
@@ -406,7 +449,7 @@
     for g in range(SIDE):
         send_one[g] = partial[g * TILE : (g + 1) * TILE].astype(BF16)
     got_one[y * tp_count + tp] = send_one[y]
-    one_here = over_plane(lambda far: send_one.at[far], got_one)
+    one_here = over_plane(lambda far: send_one.at[far, filled], got_one, lambda ref, which: ref.at[which, filled])
     loaded("gates_b")
     with jax.named_scope("plane_one"):
         one_here()
@@ -445,7 +488,11 @@
     for u in range(2):
         for h in range(2):
             zkv[z, 2 * u + h] = product[1 + u][:, h * LANES : (h + 1) * LANES].astype(BF16)
-    first_here = along_y(lambda far: first_all.at[y], lambda near: first_all.at[near], first_all.at[first_three])
+    first_here = along_y(
+        lambda far: first_all.at[y, filled],
+        lambda near: first_all.at[near, filled],
+        first_all.at[first_three, filled],
+    )
     gates_b_here = along_y(
         lambda far: gates_b.at[pl.ds(far * share, share)],
         lambda near: gates_b_all.at[:, :, near],
@@ -464,8 +511,8 @@
     query = [jnp.where(sub < GROUP, factor * both[h], 0.0).astype(BF16) for h in range(2)]
     for h in range(2):
         qf[y, h] = query[h]
-    qf_here = along_y(lambda far: qf.at[y], lambda near: qf.at[near], qf.at[first_three])
-    zkv_here = along_z(zkv)
+    qf_here = along_y(lambda far: rows_of(qf, y), lambda near: rows_of(qf, near), rows_of(qf, first_three))
+    zkv_here = along_z(zkv, rows_of)
     log_gate = []
     for h in range(2):
         gate = factor * column(line, ROWS * (h + 1)) + biases[h : h + 1]
@@ -480,7 +527,7 @@
     for k in [*y_steps, 0]:
         g = at_y(k)
         stats = jnp.zeros((1, LANES), F32)
-        pair = jnp.concatenate([qf[g, 0].astype(F32), qf[g, 1].astype(F32)]).astype(BF16)
+        pair = jnp.concatenate([jnp.where(sub < GROUP, qf[g, h].astype(F32), 0.0) for h in range(2)]).astype(BF16)
         scores = jnp.zeros((TILE, 2 * positions), F32)
         for i in range(GROUP):
             found = dot_rows(pair, keys[g * GROUP + i])
@@ -506,12 +553,12 @@
         own_stats[g] = stats
         if k:
             push(own_stats.at[g], rst.at[y], rst_sems, (z * SIDE + g, tp))
-            push(sa.at[g], ra.at[y], ra_sems, (z * SIDE + g, tp))
-    sent.append((None, ra.at[first_three], ra_sems[0]))
+            push(rows_of(sa, g), rows_of(ra, y), ra_sems, (z * SIDE + g, tp))
+    sent.append((None, rows_of(ra, first_three), ra_sems[0]))
     sent.append((None, rst.at[first_three], rst_sems[0]))
     with jax.named_scope("y_merge"):
         take(rst.at[first_three], rst_sems[1])
-        take(ra.at[first_three], ra_sems[1])
+        take(rows_of(ra, first_three), ra_sems[1])
 
     def merged(levels, parts):
         top = functools.reduce(jnp.maximum, levels)
@@ -530,7 +577,7 @@
         stats = stats + as_line(level, ROWS * h)
     zst[z] = stats
     zst_here = along_z(zst)
-    za_here = along_z(za)
+    za_here = along_z(za, rows_of)
 
     with jax.named_scope("z_keyvalue"):
         zkv_here()
@@ -556,7 +603,7 @@
     mine = dot_rows(attended, wo_all[...].reshape(slab, 2 * LANES)).astype(BF16)
     send_two[...] = mine
     got_two[y * tp_count + tp] = mine
-    two_here = over_plane(lambda far: send_two, got_two)
+    two_here = over_plane(lambda far: send_two.at[filled], got_two, lambda ref, which: ref.at[which, filled])
     with jax.named_scope("plane_two"):
         two_here()
 
@@ -583,18 +630,21 @@
         partial = jnp.zeros((ROWS, width), F32)
         for n in range(share):
             partial = partial + dot_rows(hidden[n], down_b_all[n, g])
-        send_three[g] = partial.astype(BF16)
+        send_three[g] = partial.reshape(SIDE, TILE, width).astype(BF16)
     got_three[y * tp_count + tp] = send_three[y]
-    three_here = over_plane(lambda far: send_three.at[far], got_three)
+    three_here = over_plane(lambda far: rows_of(send_three, far), got_three, rows_of)
     with jax.named_scope("plane_three"):
         three_here()
-    summed = added(got_three, 0, SIDE * tp_count)
-    last = (residual + 0.5 * summed).astype(BF16)
+    summed = added(got_three, 0, SIDE * tp_count).reshape(ROWS, width)
+    in_use = (iota((ROWS, width), 0) & 7) < GROUP
+    last = jnp.where(in_use, residual + 0.5 * summed, 0.0).astype(BF16)
 
     back = iota((seqs, ROWS), 1)
     seat = lax.shift_right_logical(back, 3) * GROUP + (back & 7)
     lift = jnp.where(((back & 7) < GROUP) & (seat == iota((seqs, ROWS), 0)), 1.0, 0.0).astype(BF16)
-    out_ref[...] = dot(lift, last).astype(BF16)
+    out_tile[...] = dot(lift, last).astype(BF16)
+    out_copy = pltpu.make_async_copy(out_tile, out_ref, fresh_sem())
+    out_copy.start()
 
     for condition, ref, sem in sent:
         if condition is None:
@@ -604,6 +654,8 @@
             @pl.when(condition)
             def _():
                 take(ref, sem)
+
+    out_copy.wait()
 
 
 def on_device(
@@ -691,7 +743,9 @@
         half(share, SIDE, width, LANES),
         half(share, 2, SIDE, width, LANES),
         half(share, SIDE, width, LANES),
-        dma((16 + 2 * (share + 21),)),
+        dma((17 + 2 * (share + 21),)),
+        (pltpu.SemaphoreType.REGULAR, pltpu.SemaphoreType.REGULAR),
+        half(seqs, width),
         half(SIDE, TILE, width),
         half(SIDE, TILE, width),
         tiles(SIDE, pieces, 2),
@@ -711,7 +765,7 @@
         ),
         (half(SIDE, TILE, slab), half(SIDE * tp_count, TILE, slab)),
         (half(TILE, slab), half(SIDE * tp_count, TILE, slab)),
-        (half(SIDE, ROWS, width), half(SIDE * tp_count, ROWS, width)),
+        (half(SIDE, SIDE, TILE, width), half(SIDE * tp_count, SIDE, TILE, width)),
         half(SIDE, TILE, slab),
         pltpu.VMEM((SIDE, TILE, 2 * length), F32),
     ]
@@ -719,7 +773,7 @@
         functools.partial(layer_kernel, ranks, width * kv_count),
         out_shape=jax.ShapeDtypeStruct(tokens.shape, BF16),
         in_specs=[pl.BlockSpec(memory_space=pltpu.HBM)] * (1 + len(operands)),
-        out_specs=pl.BlockSpec(memory_space=pltpu.VMEM),
+        out_specs=pl.BlockSpec(memory_space=pltpu.HBM),
         scratch_shapes=held,
         compiler_params=pltpu.CompilerParams(
             collective_id=0, has_side_effects=True, vmem_limit_bytes=67_043_328

time: 92.8 us -> 90.6 us (0.976)
  Pallas kernels: 91.3 us -> 89 us
    pallas_call x1, Pallas kernels: 91.3 us -> 89 us  [on_device(): pl.pallas_call(functools.partial(layer_kernel, ranks, width * kv_count),...]
where the time goes in v4:
time: 90.6 us; the launch traced here: 90.3 us
  Pallas kernels  89 us (98%)
  local copies, waits for them, and re-layouts  1.29 us (1%)
    pallas_call x1, Pallas kernels, on_device(): pl.pallas_call(functools.partial(layer_kernel, ranks, width * kv_count),...  89 us

profile of v4, /device:TPU:1, one launch (start us, length us, event | category | flops | bytes accessed | tf_op | source)
XLA Modules:
  0.0 90.3 jit_solution(2553654379895010467)
XLA Ops:
  0.0 89.0 %layer.1 = bf16[24,64]{1,0:T(8,128)(2,1)} custom-call(f32[1,16]{1,0:T(1,128)} %bitcast.16, bf16[24,64]{1,0:T(8,128)(2,1)} %tokens_hbm.1, bf16[1,64]{1,0:T(2,128)(2,1)} %bitcast.17, bf16[64,1408]{1,0:T(8,128)(2,1)} %gate_a_hbm.1, bf16[64,1408]{1,0:T(8,128)(2,1)} %up_a_hbm.1, bf16[64,1408]{1,0:T(8,128)(2,1)} %bitcast.12, bf16[1,64]{1,0:T(2,128)(2,1)} %bitcast.18, ...), custom_call_target="tpu_custom_call" | custom-call | tf_op jit(solution)/shard_map/layer/pallas_call | solution.py:772
  89.1 1.3 %copy.21 = bf16[24,64]{1,0:T(8,128)(2,1)} copy(bf16[24,64]{1,0:T(8,128)(2,1)} %layer.1) | data formatting | bytes 6144

commit v5 on v4

--- a/solution.py
+++ b/solution.py
@@ -77,7 +77,6 @@
     keys,
     values,
     decay,
-    down_a,
     gates_b,
     down_b,
     w_all,
@@ -106,7 +105,7 @@
     kv, tp = lax.axis_index("kv"), lax.axis_index("tp")
     z, y = lax.div(kv, SIDE), lax.rem(kv, SIDE)
     chunks = gate_a.shape[1] // LANES
-    share = down_a.shape[0] // SIDE
+    share = down_b.shape[0] // SIDE
     pieces = share * SIDE
     width = tokens.shape[1]
     slab = SIDE * width
@@ -179,7 +178,7 @@
     load_one("gain_b", gain_b_hbm, gain_b)
     for k in far_first(tp_count):
         signal(barrier, (z * SIDE, at_tp(k)))
-    load("down_a", down_a.at[pl.ds(0, chunks)], *[(columns(down_a_hbm, j), down_a.at[j]) for j in range(chunks)])
+    load_one("down_a", down_a_hbm, down_a_all.at[y])
     load(
         "w",
         w_all.at[:, y],
@@ -243,6 +242,14 @@
         sent.append((None, others, sems[0]))
         return lambda: take(others, sems[1])
 
+    def over_tp(target):
+        sems = fresh_pair()
+        for k in far_first(tp_count):
+            push(target.at[tp, filled], target.at[tp, filled], sems, (kv, at_tp(k)))
+        others = target.at[pl.ds(0, tp_count - 1), filled]
+        sent.append((None, others, sems[0]))
+        return lambda: take(others, sems[1])
+
     sub, lane = iota((TILE, LANES), 0), iota((TILE, LANES), 1)
 
     def column(line, first):
@@ -257,28 +264,32 @@
     def row_sum(x):
         return jnp.sum(x, axis=1, keepdims=True)
 
-    def owner(p):
-        return lax.div(p * depth, pieces)
-
-    def piece_of(place):
-        return lax.div(pieces * place + depth - 1, depth)
-
-    def owns(place):
-        p = piece_of(place)
-        return jnp.logical_and(p < pieces, owner(p) == place)
-
-    def send_pieces(bufs, sems, n):
+    def ownership(bufs):
+        count = bufs[0].shape[0]
+
+        def piece_of(place):
+            return lax.div(count * place + depth - 1, depth)
+
+        def owns(place):
+            p = piece_of(place)
+            return jnp.logical_and(p < count, lax.div(p * depth, count) == place)
+
+        return count, piece_of, owns
+
+    def send_pieces(bufs, sems, low, high):
         sz, rz, hz = bufs
+        _, piece_of, owns = ownership(bufs)
         for k in z_steps:
             far = at_z(k)
             p = piece_of(far)
 
-            @pl.when(jnp.logical_and(owns(far), lax.div(p, SIDE) == n))
+            @pl.when(owns(far) & (p >= low) & (p < high))
             def _():
                 push(sz.at[p], rz.at[z], sems, (far * SIDE + y, tp))
 
-    def hidden_units(bufs, rs_sems):
+    def hidden_units(bufs, rs_sems, group_of):
         sz, rz, hz = bufs
+        pieces, piece_of, owns = ownership(bufs)
         ag_sems = fresh_pair()
         mine_too = jnp.logical_not(owns(z))
         sent.append((owns(z), sz.at[pl.ds(0, pieces - 1)], rs_sems[0]))
@@ -295,7 +306,7 @@
                 both = both + rz[k].astype(F32)
             gate_sum, up_sum = both[0], both[1]
             factor = lax.rsqrt(gate_sum[GROUP : GROUP + 1] / features + EPSILON)
-            factor = column(factor, lax.rem(mine, SIDE) * TILE)
+            factor = column(factor, group_of(mine) * TILE)
             gate_value, up_value = factor * gate_sum, factor * up_sum
             hidden = gate_value / (1.0 + jnp.exp(-gate_value)) * up_value
             hz[mine] = jnp.where(sub < GROUP, hidden, 0.0).astype(BF16)
@@ -312,10 +323,6 @@
             @pl.when(mine_too)
             def _():
                 take(hz.at[:, filled], ag_sems[1])
-
-        return [
-            hz[n * SIDE : (n + 1) * SIDE].astype(F32).reshape(ROWS, LANES).astype(BF16) for n in range(share)
-        ]
 
     to_rows = iota((ROWS, seqs), 0)
     seat = lax.shift_right_logical(to_rows, 3) * GROUP + (to_rows & 7)
@@ -340,12 +347,8 @@
                 tile = product[g * TILE : (g + 1) * TILE, j * LANES : (j + 1) * LANES]
                 if u == 0:
                     tile = jnp.where(sub == GROUP, squares, tile)
-                sy[j // share, (j % share) * SIDE + g, u] = tile.astype(BF16)
+                sy[g, j, u] = tile.astype(BF16)
     for j in range(chunks, pieces):
-        for g in range(SIDE):
-            for u in range(2):
-                sy[j // share, (j % share) * SIDE + g, u] = jnp.zeros((TILE, LANES), BF16)
-        down_a[j] = jnp.zeros((width, LANES), BF16)
         for u in range(2):
             gates_b[j, u] = jnp.zeros((width, LANES), BF16)
         down_b[j] = jnp.zeros((width, LANES), BF16)
@@ -362,39 +365,33 @@
             pl.semaphore_wait(near_sem, len(y_steps))
 
 
+    portions = [(low, min(low + 4, chunks)) for low in range(0, chunks, 4)]
+
     def portion(ref, which, n):
-        return ref.at[which, pl.ds(n * SIDE, SIDE), :, pl.ds(0, GROUP if n else TILE)]
+        low, high = portions[n]
+        return ref.at[which, pl.ds(low, high - low), :, pl.ds(0, GROUP if n else TILE)]
 
     first_three = pl.ds(0, SIDE - 1)
     reduced = [
         along_y(lambda far: portion(sy, far, n), lambda near: portion(ry, near, n), portion(ry, first_three, n))
-        for n in range(share)
+        for n in range(len(portions))
     ]
     tiles_here = along_y(lambda far: tiles_y.at[far], lambda near: tiles_all.at[near], tiles_all.at[first_three])
     loaded("down_a")
     down_a_here = along_y(
-        lambda far: down_a.at[pl.ds(far * share, share)],
-        lambda near: down_a_all.at[:, near],
-        down_a_all.at[:, first_three],
-    )
-    down_a_all[:, y] = down_a[pl.ds(y * share, share)]
+        lambda far: down_a_all.at[y], lambda near: down_a_all.at[near], down_a_all.at[first_three]
+    )
     loaded("w")
     w_here = along_y(lambda far: w_all.at[:, y], lambda near: w_all.at[:, near], w_all.at[:, first_three])
     loaded("wo")
     wo_here = along_y(lambda far: wo_all.at[y], lambda near: wo_all.at[near], wo_all.at[first_three])
 
-    loaded("down_b")
-    down_b_here = along_y(
-        lambda far: down_b.at[pl.ds(far * share, share)],
-        lambda near: down_b_all.at[:, near],
-        down_b_all.at[:, first_three],
-    )
 
     sz, ff_sems = ff_a[0], fresh_pair()
-    for n in range(share):
+    for n, (low, high) in enumerate(portions):
         with jax.named_scope("y_reduce"):
             reduced[n]()
-        rows = pl.ds(n * SIDE, SIDE)
+        rows = pl.ds(low, high - low)
         total = sy[y, rows].astype(F32)
         for k in y_steps:
             total = total + ry[at_y(k), rows].astype(F32)
@@ -416,7 +413,7 @@
                 def _():
                     pl.semaphore_wait(far_sem, 1)
 
-        send_pieces(ff_a, ff_sems, n)
+        send_pieces(ff_a, ff_sems, low, high)
 
     loaded("decay")
     woven_all = jnp.zeros((ROWS, 2 * positions), F32)
@@ -440,16 +437,12 @@
     wide = iota((TILE, slab), 0) < GROUP
     own_rows = jnp.where(wide, own_rows, 0.0)
 
-    hidden = hidden_units(ff_a, ff_sems)
-    down_a_here()
-    partial = jnp.zeros((ROWS, slab), F32)
-    for n in range(share):
-        partial = partial + dot_rows(hidden[n], down_a_all[n].reshape(slab, LANES))
-    send_one, got_one = t_one
-    for g in range(SIDE):
-        send_one[g] = partial[g * TILE : (g + 1) * TILE].astype(BF16)
-    got_one[y * tp_count + tp] = send_one[y]
-    one_here = over_plane(lambda far: send_one.at[far, filled], got_one, lambda ref, which: ref.at[which, filled])
+    hidden_units(ff_a, ff_sems, lambda piece: y)
+    hidden = jnp.concatenate([ff_a[2][j] for j in range(chunks)], axis=1)
+    with jax.named_scope("down_wait"):
+        down_a_here()
+    t_one[tp] = dot_rows(hidden, down_a_all[...].reshape(slab, chunks * LANES)).astype(BF16)
+    one_here = over_tp(t_one)
     loaded("gates_b")
     with jax.named_scope("plane_one"):
         one_here()
@@ -460,7 +453,7 @@
             total = total + ref[first + k].astype(F32)
         return total
 
-    summed = added(got_one, 0, SIDE * tp_count)
+    summed = added(t_one, 0, tp_count)
     first_rows = (own_rows + 0.5 * summed).astype(BF16)
     first_all[y] = first_rows
 
@@ -493,10 +486,11 @@
         lambda near: first_all.at[near, filled],
         first_all.at[first_three, filled],
     )
-    gates_b_here = along_y(
-        lambda far: gates_b.at[pl.ds(far * share, share)],
-        lambda near: gates_b_all.at[:, :, near],
-        gates_b_all.at[:, :, first_three],
+    loaded("down_b")
+    down_b_here = along_y(
+        lambda far: down_b.at[pl.ds(far * share, share)],
+        lambda near: down_b_all.at[:, near],
+        down_b_all.at[:, first_three],
     )
     gates_b_all[:, :, y] = gates_b[pl.ds(y * share, share)]
     down_b_all[:, y] = down_b[pl.ds(y * share, share)]
@@ -511,7 +505,10 @@
     query = [jnp.where(sub < GROUP, factor * both[h], 0.0).astype(BF16) for h in range(2)]
     for h in range(2):
         qf[y, h] = query[h]
-    qf_here = along_y(lambda far: rows_of(qf, y), lambda near: rows_of(qf, near), rows_of(qf, first_three))
+    query_sems = {k: fresh_pair() for k in y_steps}
+    for k in y_steps:
+        push(rows_of(qf, y), rows_of(qf, y), query_sems[k], (z * SIDE + at_y(k), tp))
+        sent.append((None, rows_of(qf, y), query_sems[k][0]))
     zkv_here = along_z(zkv, rows_of)
     log_gate = []
     for h in range(2):
@@ -519,13 +516,14 @@
         log_gate.append(jnp.minimum(gate, 0.0) - jnp.log(1.0 + jnp.exp(-jnp.abs(gate))))
     loaded("keys", "values")
 
-    with jax.named_scope("y_query"):
-        qf_here()
     lane2, sub2 = iota((TILE, 2 * positions), 1), iota((TILE, 2 * positions), 0)
     even = lax.rem(lane2, 2) == 0
     ra_sems, rst_sems = fresh_pair(), fresh_pair()
-    for k in [*y_steps, 0]:
+    for k in [0, *reversed(y_steps)]:
         g = at_y(k)
+        if k:
+            with jax.named_scope("y_query"):
+                take(rows_of(qf, g), query_sems[SIDE - k][1])
         stats = jnp.zeros((1, LANES), F32)
         pair = jnp.concatenate([jnp.where(sub < GROUP, qf[g, h].astype(F32), 0.0) for h in range(2)]).astype(BF16)
         scores = jnp.zeros((TILE, 2 * positions), F32)
@@ -579,6 +577,12 @@
     zst_here = along_z(zst)
     za_here = along_z(za, rows_of)
 
+    gates_b_here = along_y(
+        lambda far: gates_b.at[pl.ds(far * share, share)],
+        lambda near: gates_b_all.at[:, :, near],
+        gates_b_all.at[:, :, first_three],
+    )
+
     with jax.named_scope("z_keyvalue"):
         zkv_here()
     both = zkv[0].astype(F32)
@@ -621,10 +625,13 @@
                 if u == 0:
                     tile = jnp.where(sub == GROUP, squares, tile)
                 sz[n * SIDE + g, u] = tile.astype(BF16)
-        send_pieces(ff_b, ff_sems, n)
+        send_pieces(ff_b, ff_sems, n * SIDE, (n + 1) * SIDE)
     lower = jnp.where(iota((slab, width), 0) == iota((slab, width), 1) + y * width, 1.0, 0.0).astype(BF16)
     residual = dot(mixed.astype(BF16), lower)
-    hidden = hidden_units(ff_b, ff_sems)
+    hidden_units(ff_b, ff_sems, lambda piece: lax.rem(piece, SIDE))
+    hidden = [
+        ff_b[2][n * SIDE : (n + 1) * SIDE].astype(F32).reshape(ROWS, LANES).astype(BF16) for n in range(share)
+    ]
     send_three, got_three = t_three
     for g in range(SIDE):
         partial = jnp.zeros((ROWS, width), F32)
@@ -720,8 +727,8 @@
     def tiles(*dims):
         return pltpu.VMEM((*dims, TILE, LANES), BF16)
 
-    def ff():
-        return (tiles(pieces, 2), tiles(depth, 2), tiles(pieces))
+    def ff(count):
+        return (tiles(count, 2), tiles(depth, 2), tiles(count))
 
     held = [
         pltpu.VMEM((1, forget_weight.shape[1]), F32),
@@ -735,23 +742,22 @@
         half(seqs, 2 * length, LANES),
         half(seqs, 2 * length, LANES),
         pltpu.VMEM(forget_sum.shape, F32),
-        half(pieces, width, LANES),
         half(pieces, 2, width, LANES),
         half(pieces, width, LANES),
         half(3, SIDE, width, 2 * LANES),
         half(SIDE, width, 2 * LANES),
-        half(share, SIDE, width, LANES),
+        half(SIDE, width, chunks * LANES),
         half(share, 2, SIDE, width, LANES),
         half(share, SIDE, width, LANES),
-        dma((17 + 2 * (share + 21),)),
+        dma((17 + 2 * (-(-chunks // 4) + 23),)),
         (pltpu.SemaphoreType.REGULAR, pltpu.SemaphoreType.REGULAR),
         half(seqs, width),
         half(SIDE, TILE, width),
         half(SIDE, TILE, width),
-        tiles(SIDE, pieces, 2),
-        tiles(SIDE, pieces, 2),
-        ff(),
-        ff(),
+        tiles(SIDE, chunks, 2),
+        tiles(SIDE, chunks, 2),
+        ff(chunks),
+        ff(pieces),
         (
             tiles(depth, 2),
             tiles(depth, 4),
@@ -763,7 +769,7 @@
             tiles(depth, 2),
             pltpu.VMEM((depth, 1, LANES), F32),
         ),
-        (half(SIDE, TILE, slab), half(SIDE * tp_count, TILE, slab)),
+        half(tp_count, TILE, slab),
         (half(TILE, slab), half(SIDE * tp_count, TILE, slab)),
         (half(SIDE, SIDE, TILE, width), half(SIDE * tp_count, SIDE, TILE, width)),
         half(SIDE, TILE, slab),

time: 90.6 us -> 89.4 us (0.987)
  Pallas kernels: 89 us -> 87.9 us
    pallas_call x1, Pallas kernels: 89 us -> 87.9 us  [on_device(): pl.pallas_call(functools.partial(layer_kernel, ranks, width * kv_count),...]
where the time goes in v5:
time: 89.4 us; the launch traced here: 89.2 us
  Pallas kernels  87.9 us (98%)
  local copies, waits for them, and re-layouts  1.29 us (1%)
    pallas_call x1, Pallas kernels, on_device(): pl.pallas_call(functools.partial(layer_kernel, ranks, width * kv_count),...  87.9 us

profile of v5, /device:TPU:1, one launch (start us, length us, event | category | flops | bytes accessed | tf_op | source)
XLA Modules:
  0.0 89.2 jit_solution(3288771097406265027)
XLA Ops:
  0.0 87.9 %layer.1 = bf16[24,64]{1,0:T(8,128)(2,1)} custom-call(f32[1,16]{1,0:T(1,128)} %bitcast.16, bf16[24,64]{1,0:T(8,128)(2,1)} %tokens_hbm.1, bf16[1,64]{1,0:T(2,128)(2,1)} %bitcast.17, bf16[64,1408]{1,0:T(8,128)(2,1)} %gate_a_hbm.1, bf16[64,1408]{1,0:T(8,128)(2,1)} %up_a_hbm.1, bf16[64,1408]{1,0:T(8,128)(2,1)} %bitcast.12, bf16[1,64]{1,0:T(2,128)(2,1)} %bitcast.18, ...), custom_call_target="tpu_custom_call" | custom-call | tf_op jit(solution)/shard_map/layer/pallas_call | solution.py:778
  88.0 1.3 %copy.21 = bf16[24,64]{1,0:T(8,128)(2,1)} copy(bf16[24,64]{1,0:T(8,128)(2,1)} %layer.1) | data formatting | bytes 6144

commit v6 on v5

--- a/solution.py
+++ b/solution.py
@@ -225,13 +225,23 @@
         sent.append((None, three, sems[0]))
         return lambda: take(three, sems[1])
 
-    def along_z(target, view=lambda ref, which: ref.at[which]):
-        sems = fresh_pair()
+    def whole_of(ref, which):
+        return ref.at[which]
+
+    def along_z_together(*targets):
+        pairs = [fresh_pair() for _ in targets]
         for k in z_steps:
-            push(view(target, z), view(target, z), sems, (at_z(k) * SIDE + y, tp))
-        others = view(target, pl.ds(0, depth - 1))
-        sent.append((None, others, sems[0]))
-        return lambda: take(others, sems[1])
+            for (target, view), sems in zip(targets, pairs):
+                push(view(target, z), view(target, z), sems, (at_z(k) * SIDE + y, tp))
+        arrivals = []
+        for (target, view), sems in zip(targets, pairs):
+            others = view(target, pl.ds(0, depth - 1))
+            sent.append((None, others, sems[0]))
+            arrivals.append(functools.partial(take, others, sems[1]))
+        return arrivals
+
+    def along_z(target, view=whole_of):
+        return along_z_together((target, view))[0]
 
     def over_plane(source_of, target, view):
         sems = fresh_pair()
@@ -574,8 +584,7 @@
         za[z, h] = value.astype(BF16)
         stats = stats + as_line(level, ROWS * h)
     zst[z] = stats
-    zst_here = along_z(zst)
-    za_here = along_z(za, rows_of)
+    za_here, zst_here = along_z_together((za, rows_of), (zst, whole_of))
 
     gates_b_here = along_y(
         lambda far: gates_b.at[pl.ds(far * share, share)],

time: 89.4 us -> 89.5 us (level)
  no operation moved by 1% of the time
where the time goes in v6:
time: 89.5 us; the launch traced here: 89.3 us
  Pallas kernels  88 us (98%)
  local copies, waits for them, and re-layouts  1.29 us (1%)
    pallas_call x1, Pallas kernels, on_device(): pl.pallas_call(functools.partial(layer_kernel, ranks, width * kv_count),...  88 us

profile of v6, /device:TPU:1, one launch (start us, length us, event | category | flops | bytes accessed | tf_op | source)
XLA Modules:
  0.0 89.3 jit_solution(1068357614618283407)
XLA Ops:
  0.0 88.0 %layer.1 = bf16[24,64]{1,0:T(8,128)(2,1)} custom-call(f32[1,16]{1,0:T(1,128)} %bitcast.16, bf16[24,64]{1,0:T(8,128)(2,1)} %tokens_hbm.1, bf16[1,64]{1,0:T(2,128)(2,1)} %bitcast.17, bf16[64,1408]{1,0:T(8,128)(2,1)} %gate_a_hbm.1, bf16[64,1408]{1,0:T(8,128)(2,1)} %up_a_hbm.1, bf16[64,1408]{1,0:T(8,128)(2,1)} %bitcast.12, bf16[1,64]{1,0:T(2,128)(2,1)} %bitcast.18, ...), custom_call_target="tpu_custom_call" | custom-call | tf_op jit(solution)/shard_map/layer/pallas_call | solution.py:787
  88.0 1.3 %copy.21 = bf16[24,64]{1,0:T(8,128)(2,1)} copy(bf16[24,64]{1,0:T(8,128)(2,1)} %layer.1) | data formatting | bytes 6144
